TPU v7x, 32 devices: a whole 2x2x4 slice. The times are simulated.
32 devices in a mesh: grp: 2 (over x), ep: 4 (over y, core), tp: 4 (over z).
Axes of the slice: x: 2, y: 2, z: 4, core: 2. Of those that a mesh axis runs over, the one named last changes fastest.
Arguments:
- tokens: bfloat16 [512, 2048], P(('grp', 'ep')), parts along dimension 0, may hold values from -6 to 6
- routing: int32 [512, 4], P(('grp', 'ep')), parts along dimension 0, may hold values from 0 to 7, all different within a row; in each aligned block of 64 rows (0 to 63, 64 to 127, ...) at most 64 rows name the same one
- route_weight: float32 [512, 4], P(('grp', 'ep')), parts along dimension 0, may hold values from 0.1 to 1
- norm_gain: float32 [2048], replicated, may hold values from 0.1 to 1.9
- gate_weight: bfloat16 [8, 2048, 2048], P('ep', None, 'tp'), may hold values from -2.1213203 to 2.1213203
- up_weight: bfloat16 [8, 2048, 2048], P('ep', None, 'tp'), may hold values from -2.1213203 to 2.1213203
- down_weight: bfloat16 [8, 2048, 2048], P('ep', 'tp'), may hold values from -3.9774756 to 3.9774756
- out_gain: float32 [2048], P('tp'), may hold values from 0.1 to 1.9
Outputs:
- layer_output: bfloat16 [512, 2048], P(('grp', 'ep'), 'tp'), parts along dimension 0
There are 2 independent parts, one for each index of `grp`. A program takes and returns all parts, laid end to end along the dimension named above; an argument that names none is the same for every part. Nothing has to cross between parts.
Inputs may be any that keep to these rules, and one draw needn't show every extreme that they name: `routing`: each row names 4 different experts; among the 64 rows of one index of ep no expert is named more than 64 times, and in some such blocks one expert is named exactly 64 times.
All inputs are finite; a program needn't handle non-finite values.
Results may differ from a plain program's by a relative error of at most 0.017.
Values may be sent and summed in bfloat16 or wider, within the bound.
No kernel may reach another device: no remote copies, remote signals or barrier semaphores. Data moves between devices by JAX's collectives and lax.ppermute only.
A program may use at most 64 MiB of HBM per device.

v0:
```python
import jax
import jax.numpy as jnp
from jax import lax
from jax.sharding import PartitionSpec as P

LIMIT = 7.0
ALPHA = 1.702
EPS = 1e-06


def slot_ranks(blocks):
    assign_count = blocks.shape[1]
    same_expert = blocks[:, :, None] == blocks[:, None, :]
    position = jnp.arange(assign_count, dtype=jnp.int32)
    earlier = position[None, :] < position[:, None]
    counted = jnp.where(same_expert & earlier[None, :, :], 1, 0).astype(jnp.int32)
    return jnp.sum(counted, axis=2)


def run_experts(expert_rows, gate_weight, up_weight, down_weight):
    gate_act = jnp.minimum(
        jnp.einsum("erd,edf->erf", expert_rows, gate_weight, preferred_element_type=jnp.float32),
        LIMIT,
    )
    up_act = jnp.clip(
        jnp.einsum("erd,edf->erf", expert_rows, up_weight, preferred_element_type=jnp.float32),
        -LIMIT,
        LIMIT,
    )
    hidden = ((up_act + 1.0) * gate_act * jax.nn.sigmoid(ALPHA * gate_act)).astype(jnp.bfloat16)
    partial_terms = jnp.einsum(
        "erf,efd->erd", hidden, down_weight, preferred_element_type=jnp.float32
    )
    summed = lax.psum_scatter(
        partial_terms.astype(jnp.bfloat16), "tp", scatter_dimension=2, tiled=True
    )
    return summed


def on_device(
    tokens, routing, route_weight, norm_gain, gate_weight, up_weight, down_weight, out_gain
):
    tok_count, model_width = tokens.shape
    top_count = routing.shape[1]
    ep_size = lax.axis_size("ep")
    local_experts = gate_weight.shape[0]
    all_experts = local_experts * ep_size
    capacity = 2 * tok_count * top_count // all_experts
    rows_per_expert = ep_size * capacity
    assign_count = tok_count * top_count
    scaled = tokens.astype(jnp.float32)
    normed = (
        scaled * lax.rsqrt(jnp.mean(scaled * scaled, axis=-1, keepdims=True) + EPS) * norm_gain
    ).astype(jnp.bfloat16)
    flat_route = routing.reshape(assign_count)
    slot_rank = slot_ranks(flat_route[None, :])[0]
    slot_index = flat_route * capacity + slot_rank
    slot_total = all_experts * capacity
    onehot = (jnp.arange(slot_total, dtype=jnp.int32)[:, None] == slot_index[None, :]).astype(
        jnp.bfloat16
    )
    repeated = jnp.repeat(normed, top_count, axis=0)
    outgoing = jnp.dot(onehot, repeated, preferred_element_type=jnp.float32).astype(jnp.bfloat16)
    outgoing = outgoing.reshape(ep_size, local_experts, capacity, model_width)
    incoming = lax.all_to_all(outgoing, "ep", split_axis=0, concat_axis=2, tiled=True)
    expert_rows = incoming.reshape(local_experts, rows_per_expert, model_width)
    expert_out = run_experts(expert_rows, gate_weight, up_weight, down_weight)
    out_width = expert_out.shape[2]
    returning = expert_out.reshape(1, local_experts, rows_per_expert, out_width)
    arrived = lax.all_to_all(returning, "ep", split_axis=2, concat_axis=0, tiled=True)
    arrived = arrived.reshape(slot_total, out_width)
    picked_rows = arrived[slot_index].astype(jnp.float32)
    gate_value = route_weight.reshape(assign_count)
    expert_mix = jnp.sum(
        (picked_rows * gate_value[:, None]).reshape(tok_count, top_count, out_width), axis=1
    )
    square_sum = lax.psum(jnp.sum(expert_mix * expert_mix, axis=1), "tp")
    scale_factor = lax.rsqrt(square_sum / model_width + EPS)
    return (expert_mix * scale_factor[:, None] * out_gain).astype(jnp.bfloat16)


def solution(mesh):
    in_specs = (
        P(("grp", "ep"), None),
        P(("grp", "ep"), None),
        P(("grp", "ep"), None),
        P(),
        P("ep", None, "tp"),
        P("ep", None, "tp"),
        P("ep", "tp", None),
        P("tp"),
    )
    out_specs = P(("grp", "ep"), "tp")
    return jax.shard_map(
        on_device, mesh=mesh, in_specs=in_specs, out_specs=out_specs, check_vma=False
    )
```

profile of v0, /device:TPU:0, one launch (start us, length us, event | category | flops | bytes accessed | tf_op | source)
XLA Modules:
  0.0 128.5 jit_solution(13875056763938892923)
XLA Ops:
  6.5 0.0 reduce-scatter.2.cloned.1.call-start
  6.5 0.8 copy.23
  7.3 0.1 reshape.164
  7.4 0.2 select_reduce_fusion
  7.6 1.1 fusion.4
  8.7 1.1 fusion.6
  9.8 0.5 broadcast_in_dim.12
  10.3 0.3 reshape.165
  10.6 0.7 convolution_convert_fusion.1
  11.3 0.0 copy-start.3
  11.4 30.0 %all_to_all.30 = bf16[4,2,64,2048]{3,2,1,0:T(8,128)(2,1)S(1)} all-to-all(bf16[4,2,64,2048]{3,2,1,0:T(8,128)(2,1)S(1)} %bitcast.19), channel_id=1, replica_groups=mesh['grp'=2,'ep'=4,'tp'=4] {'ep'}, dimensions={0} | all-to-all | bytes 4194304 | tf_op jit(solution)/shard_map/all_to_all | solution.py:65
  41.4 0.1 copy.24
  41.5 0.0 copy-done.3
  41.5 1.2 convolution_minimum_fusion
  42.8 7.3 %convolution_convert_fusion = bf16[2,256,2048]{2,1,0:T(8,128)(2,1)} fusion(bf16[2,512,2048]{2,1,0:T(8,128)(2,1)} %param.14, f32[2,256,512]{2,1,0:T(8,128)S(1)} %convolution_minimum_fusion, bf16[2,256,2048]{2,1,0:T(8,128)(2,1)S(1)} %bitcast.22, bf16[2,2048,512]{2,1,0:T(8,128)(2,1)} %param.13), kind=kOutput, calls=%fused_computation.1 | convolution fusion | flops 2150891520 | bytes 13631488 | tf_op jit(solution)/shard_map/erf,efd->erd/dot_general | solution.py:31
  50.1 0.0 copy-start
  50.1 0.0 copy-start.2
  50.1 0.0 copy-start.1
  50.1 0.0 reduce-scatter.2.cloned.1.call-update
  50.1 44.1 %reduce-scatter.2.cloned.1.call-done = bf16[2,256,512]{2,1,0:T(8,128)(2,1)} async-done(((bf16[2,256,2048]{2,1,0:T(8,128)(2,1)}), bf16[2,256,512]{2,1,0:T(8,128)(2,1)}) %reduce-scatter.2.cloned.1.call-update) | async-done | bytes 524304 | tf_op jit(solution)/shard_map/reduce_scatter | solution.py:34
  94.2 2.4 %copy.25 = bf16[1,2,256,512]{3,1,0,2:T(2,128)(2,1)} copy(bf16[1,2,256,512]{3,2,1,0:T(8,128)(2,1)} %bitcast.24) | data formatting | bytes 1048576 | tf_op jit(solution)/shard_map/reshape | solution.py:69
  96.6 3.5 %all-to-all-start.1 = ((bf16[1,2,256,512]{3,1,0,2:T(2,128)(2,1)}), bf16[1,2,256,512]{3,1,0,2:T(2,128)(2,1)S(1)}, u32[]{:S(2)}, u32[]{:S(2)}) async-start(bf16[1,2,256,512]{3,1,0,2:T(2,128)(2,1)} %copy.25), calls=%async_computation.2 | async-start | bytes 1048576 | tf_op jit(solution)/shard_map/all_to_all | solution.py:70
  100.0 0.0 copy-done
  100.1 0.1 copy.27
  100.2 0.1 mul.96
  100.3 0.0 copy-done.2
  100.3 0.1 copy.28
  100.4 8.4 %all-to-all-done.1 = bf16[1,2,256,512]{3,1,0,2:T(2,128)(2,1)S(1)} async-done(((bf16[1,2,256,512]{3,1,0,2:T(2,128)(2,1)}), bf16[1,2,256,512]{3,1,0,2:T(2,128)(2,1)S(1)}, u32[]{:S(2)}, u32[]{:S(2)}) %all-to-all-start.1) | async-done | bytes 524320 | tf_op jit(solution)/shard_map/all_to_all | solution.py:70
  108.8 0.1 copy.26
  108.9 1.2 gather_fusion
  110.0 0.2 reshape.170
  110.2 0.4 multiply_reduce_fusion
  110.6 0.1 multiply_reduce_fusion.1
  110.7 10.2 %psum.7 = f32[64]{0:T(128)S(1)} all-reduce(f32[64]{0:T(128)S(1)} %multiply_reduce_fusion.1), channel_id=1, replica_groups=mesh['grp'=2,'ep'=4,'tp'=4] {'tp'}, use_global_device_ids=true, to_apply=%region_5.6 | all-reduce | flops 64 | bytes 512 | tf_op jit(solution)/shard_map/psum | solution.py:77
  120.9 0.0 copy-done.1
  120.9 0.7 multiply_convert_fusion
  (6 shorter events, 0.0 us)
Async XLA Ops:
  6.5 87.7 %reduce-scatter.2.cloned.1.call-start = ((), (), s32[]{:S(2)}) async-start(), calls=%async_computation.3 | async-start | bytes 2621440 | tf_op jit(solution)/shard_map/reduce_scatter | solution.py:34
  11.3 30.2 %copy-start.3 = (bf16[2,2048,512]{2,1,0:T(8,128)(2,1)S(1)}, bf16[2,2048,512]{2,1,0:T(8,128)(2,1)}, u32[]{:S(2)}) copy-start(bf16[2,2048,512]{2,1,0:T(8,128)(2,1)} %param.12) | copy-start | bytes 12582916
  50.1 49.9 %copy-start = (s32[64,4]{0,1:T(4,128)S(1)}, s32[64,4]{0,1:T(4,128)}, u32[]{:S(2)}) copy-start(s32[64,4]{0,1:T(4,128)} %param.9) | copy-start | bytes 3076
  50.1 50.2 %copy-start.2 = (f32[64,4]{0,1:T(4,128)S(1)}, f32[64,4]{0,1:T(4,128)}, u32[]{:S(2)}) copy-start(f32[64,4]{0,1:T(4,128)} %param.10) | copy-start | bytes 3076
  50.1 70.8 %copy-start.1 = (f32[512]{0:T(512)S(1)}, f32[512]{0:T(512)}, u32[]{:S(2)}) copy-start(f32[512]{0:T(512)} %param.15) | copy-start | bytes 6148
  96.6 12.3 %all-to-all-start.1 = ((bf16[1,2,256,512]{3,1,0,2:T(2,128)(2,1)}), bf16[1,2,256,512]{3,1,0,2:T(2,128)(2,1)S(1)}, u32[]{:S(2)}, u32[]{:S(2)}) async-start(bf16[1,2,256,512]{3,1,0,2:T(2,128)(2,1)} %copy.25), calls=%async_computation.2 | async-start | bytes 1048576 | tf_op jit(solution)/shard_map/all_to_all | solution.py:70
Sparse Core Ops, SparseCore 0:
  50.3 43.9 reduce-scatter.1
where the time goes:
time: 129 us; the launch traced here: 128 us
  waiting for transfers between devices  52.5 us (41%)
  blocking collectives  40.2 us (31%)
  between operations  13.5 us (10%)
  matrix products  9.3 us (7%)
  local copies, waits for them, and re-layouts  5.85 us (5%)
  other arithmetic  3.63 us (3%)
  starting transfers between devices  3.47 us (3%)
    reduce_scatter x1, waiting for transfers between devices, run_experts(): lax.psum_scatter(partial_terms.astype(jnp.bfloat16), 'tp', scatter_dimens...  44.1 us
    all_to_all x1, blocking collectives, on_device(): lax.all_to_all(outgoing, 'ep', split_axis=0, concat_axis=2, tiled=True)  30 us
    psum x1, blocking collectives, on_device(): square_sum = lax.psum(jnp.sum(expert_mix * expert_mix, axis=1), 'tp')  10.2 us
    all_to_all x1, waiting for transfers between devices, on_device(): lax.all_to_all(returning, 'ep', split_axis=2, concat_axis=0, tiled=True)  8.43 us
    dot_general x1, matrix products, run_experts(): jnp.einsum('erf,efd->erd', hidden, down_weight, preferred_element_type=jn...  7.34 us
    all_to_all x1, starting transfers between devices, on_device(): lax.all_to_all(returning, 'ep', split_axis=2, concat_axis=0, tiled=True)  3.47 us
  transfers between devices with their start and end apart: 2, of which 2 were waited for; matrix products, arithmetic and copies ran while one was open for 0% of the time, Pallas kernels for 0%

commit v1 on v0

v1 whole, which is shorter than its diff:
```python
import functools

import jax
import jax.numpy as jnp
from jax import lax
from jax.experimental import pallas as pl
from jax.experimental.pallas import tpu as pltpu
from jax.sharding import PartitionSpec as P

LIMIT = 7.0
ALPHA = 1.702
EPS = 1e-06
LANES = 128


def pack_kernel(tok_ref, route_ref, weight_ref, gain_ref, out_ref, *, half):
    width = tok_ref.shape[1]
    scaled = tok_ref[...].astype(jnp.float32)
    mean = jnp.mean(scaled * scaled, axis=-1, keepdims=True)
    out_ref[:, :width] = (scaled * lax.rsqrt(mean + EPS) * gain_ref[...]).astype(jnp.bfloat16)
    rows = tok_ref.shape[0]
    lane = lax.broadcasted_iota(jnp.int32, (rows, 2 * half), 1)
    expert = jnp.where(lane < half, lane, lane - half)
    dense = jnp.zeros((rows, 2 * half), jnp.float32)
    for k in range(route_ref.shape[1]):
        dense += jnp.where(route_ref[:, k : k + 1] == expert, weight_ref[:, k : k + 1], 0.0)
    high = dense.astype(jnp.bfloat16).astype(jnp.float32)
    out_ref[:, width:] = jnp.where(lane < half, high, dense - high).astype(jnp.bfloat16)


def pack(tokens, routing, route_weight, norm_gain, half):
    rows, width = tokens.shape
    return pl.pallas_call(
        functools.partial(pack_kernel, half=half),
        out_shape=jax.ShapeDtypeStruct((rows, width + 2 * half), jnp.bfloat16),
        name="pack",
    )(tokens, routing, route_weight, norm_gain.reshape(1, width))


def moe_kernel(place_ref, *refs, blocks, half, chunks):
    x_refs = refs[:blocks]
    gate_ref, up_ref, down_ref, keep_ref, send_ref, x_all, w_all, acc = refs[blocks:]
    step = pl.program_id(0)
    rows = x_refs[0].shape[0]
    width = x_all.shape[1]

    @pl.when(step == 0)
    def _():
        for b in range(blocks):
            x_all[b * rows : (b + 1) * rows, :] = x_refs[b][:, :width]
            w_all[b * rows : (b + 1) * rows, :] = x_refs[b][:, width:].astype(jnp.float32)

    expert = place_ref[0] + step // chunks
    lane = lax.broadcasted_iota(jnp.int32, w_all.shape, 1)
    mine = (lane == expert) | (lane == expert + half)
    weight = jnp.sum(jnp.where(mine, w_all[...], 0.0), axis=1, keepdims=True)
    x = x_all[...]
    gate = jnp.minimum(jnp.dot(x, gate_ref[0], preferred_element_type=jnp.float32), LIMIT)
    up = jnp.clip(jnp.dot(x, up_ref[0], preferred_element_type=jnp.float32), -LIMIT, LIMIT)
    hidden = ((up + 1.0) * gate * jax.nn.sigmoid(ALPHA * gate) * weight).astype(jnp.bfloat16)
    part = jnp.dot(hidden, down_ref[0], preferred_element_type=jnp.float32)

    @pl.when(step == 0)
    def _():
        acc[...] = part

    @pl.when(step > 0)
    def _():
        acc[...] += part

    @pl.when(step == pl.num_programs(0) - 1)
    def _():
        for b in range(blocks // 2):
            keep_ref[b] = acc[2 * b * rows : (2 * b + 1) * rows, :].astype(jnp.bfloat16)
            send_ref[b] = acc[(2 * b + 1) * rows : (2 * b + 2) * rows, :].astype(jnp.bfloat16)


def run_experts(x_blocks, gate_weight, up_weight, down_weight, place, half):
    blocks = len(x_blocks)
    rows, packed = x_blocks[0].shape
    experts, width, hidden = gate_weight.shape
    chunk = min(hidden, 256)
    chunks = hidden // chunk
    out = jax.ShapeDtypeStruct((blocks // 2, rows, width), jnp.bfloat16)
    whole = lambda shape: pl.BlockSpec(shape, lambda s, p: (0,) * len(shape))
    return pl.pallas_call(
        functools.partial(moe_kernel, blocks=blocks, half=half, chunks=chunks),
        grid_spec=pltpu.PrefetchScalarGridSpec(
            num_scalar_prefetch=1,
            grid=(experts * chunks,),
            in_specs=[whole((rows, packed))] * blocks
            + [
                pl.BlockSpec((1, width, chunk), lambda s, p: (s // chunks, 0, s % chunks)),
                pl.BlockSpec((1, width, chunk), lambda s, p: (s // chunks, 0, s % chunks)),
                pl.BlockSpec((1, chunk, width), lambda s, p: (s // chunks, s % chunks, 0)),
            ],
            out_specs=[whole(out.shape)] * 2,
            scratch_shapes=[
                pltpu.VMEM((blocks * rows, width), jnp.bfloat16),
                pltpu.VMEM((blocks * rows, 2 * half), jnp.float32),
                pltpu.VMEM((blocks * rows, width), jnp.float32),
            ],
        ),
        out_shape=[out, out],
        name="experts",
    )(place, *x_blocks, gate_weight, up_weight, down_weight)


def swap(value, axis, size, bit):
    return lax.ppermute(value, axis, [(s, s ^ bit) for s in range(size)])


def shift(value, axis, size, amount):
    return lax.ppermute(value, axis, [(s, (s + amount) % size) for s in range(size)])


def on_device(
    ep_size, tp_size,
    tokens, routing, route_weight, norm_gain, gate_weight, up_weight, down_weight, out_gain
):
    model_width = tokens.shape[1]
    local_experts = gate_weight.shape[0]
    all_experts = local_experts * ep_size
    half = -(-all_experts // 64) * 64
    ep_index = lax.axis_index("ep")
    tp_index = lax.axis_index("tp")
    bits = [1 << b for b in range(ep_size.bit_length() - 1)]

    arrived = {0: pack(tokens, routing, route_weight, norm_gain, half)}
    for bit in reversed(bits):
        for j in list(arrived):
            arrived[j ^ bit] = swap(arrived[j], "ep", ep_size, bit)
    x_blocks = [arrived[j] for j in range(ep_size)]
    place = (ep_index * local_experts).astype(jnp.int32).reshape(1)
    keep, send = run_experts(x_blocks, gate_weight, up_weight, down_weight, place, half)
    for bit in bits:
        got = swap(send, "ep", ep_size, bit)
        total = keep.astype(jnp.float32) + got.astype(jnp.float32)
        if bit == bits[-1]:
            mixed = total[0].astype(jnp.bfloat16)
        else:
            keep = total[0::2].astype(jnp.bfloat16)
            send = total[1::2].astype(jnp.bfloat16)
    out_width = model_width // tp_size
    block = lambda d: lax.dynamic_slice_in_dim(
        mixed, ((tp_index + d) % tp_size) * out_width, out_width, axis=1
    )
    expert_mix = block(0).astype(jnp.float32)
    for d in range(1, tp_size):
        expert_mix += shift(block(d), "tp", tp_size, d).astype(jnp.float32)
    square = jnp.sum(expert_mix * expert_mix, axis=1)
    square_sum = square
    for d in range(1, tp_size):
        square_sum += shift(square, "tp", tp_size, d)
    scale_factor = lax.rsqrt(square_sum / model_width + EPS)
    return (expert_mix * scale_factor[:, None] * out_gain).astype(jnp.bfloat16)


def solution(mesh):
    in_specs = (
        P(("grp", "ep"), None),
        P(("grp", "ep"), None),
        P(("grp", "ep"), None),
        P(),
        P("ep", None, "tp"),
        P("ep", None, "tp"),
        P("ep", "tp", None),
        P("tp"),
    )
    out_specs = P(("grp", "ep"), "tp")
    return jax.shard_map(
        functools.partial(on_device, mesh.shape["ep"], mesh.shape["tp"]),
        mesh=mesh, in_specs=in_specs, out_specs=out_specs, check_vma=False
    )
```

time: 129 us -> 56.4 us (0.44)
  blocking collectives: 40.2 us -> 0 us
  waiting for transfers between devices: 52.5 us -> 25.5 us
  between operations: 13.5 us -> 0.06 us
  Pallas kernels: 0 us -> 11.4 us
  starting transfers between devices: 3.47 us -> 13.5 us
  matrix products: 9.3 us -> 0 us
  local copies, waits for them, and re-layouts: 5.85 us -> 3.55 us
  other arithmetic: 3.63 us -> 2.09 us
    reduce_scatter x1 -> x0, waiting for transfers between devices: 44.1 us -> none  [run_experts(): lax.psum_scatter(partial_terms.astype(jnp.bfloat16), 'tp', scatter_dimens...]
    all_to_all x1 -> x0, blocking collectives: 30 us -> none  [on_device(): lax.all_to_all(outgoing, 'ep', split_axis=0, concat_axis=2, tiled=True)]
    ppermute x0 -> x11, waiting for transfers between devices: none -> 25.5 us  [the longest x5 17 us: swap(): return lax.ppermute(value, axis, [(s, s ^ bit) for s in range(size)])]
    ppermute x0 -> x11, starting transfers between devices: none -> 13.5 us  [the longest x6 8.58 us: shift(): lax.ppermute(value, axis, [(s, (s + amount) % size) for s in range(size)])]
    pallas_call x0 -> x2, Pallas kernels: none -> 11.4 us  [the longest x1 9.49 us: run_experts(): pl.pallas_call(functools.partial(moe_kernel, blocks=blocks, half=half, ch...]
    psum x1 -> x0, blocking collectives: 10.2 us -> none  [on_device(): square_sum = lax.psum(jnp.sum(expert_mix * expert_mix, axis=1), 'tp')]
    dot_general x3 -> x0, matrix products: 9.3 us -> none  [the longest x1 7.34 us: run_experts(): jnp.einsum('erf,efd->erd', hidden, down_weight, preferred_element_type=jn...]
    all_to_all x1 -> x0, waiting for transfers between devices: 8.43 us -> none  [on_device(): lax.all_to_all(returning, 'ep', split_axis=2, concat_axis=0, tiled=True)]
  transfers between devices with their start and end apart: 2 -> 11, of which waited for: 2 -> 9; matrix products, arithmetic and copies ran while one was open for 0% -> 0% of each run, Pallas kernels for 0% -> 0%
where the time goes in v1:
time: 56.4 us; the launch traced here: 56.2 us
  waiting for transfers between devices  25.5 us (45%)
  starting transfers between devices  13.5 us (24%)
  Pallas kernels  11.4 us (20%)
  local copies, waits for them, and re-layouts  3.55 us (6%)
  other arithmetic  2.09 us (4%)
    ppermute x5, waiting for transfers between devices, swap(): return lax.ppermute(value, axis, [(s, s ^ bit) for s in range(size)])  17 us
    pallas_call x1, Pallas kernels, run_experts(): pl.pallas_call(functools.partial(moe_kernel, blocks=blocks, half=half, ch...  9.49 us
    ppermute x6, starting transfers between devices, shift(): lax.ppermute(value, axis, [(s, (s + amount) % size) for s in range(size)])  8.58 us
    ppermute x6, waiting for transfers between devices, shift(): lax.ppermute(value, axis, [(s, (s + amount) % size) for s in range(size)])  8.53 us
    ppermute x5, starting transfers between devices, swap(): return lax.ppermute(value, axis, [(s, s ^ bit) for s in range(size)])  4.96 us
    unnamed x10, local copies, waits for them, and re-layouts  3.5 us
    pallas_call x1, Pallas kernels, pack(): pl.pallas_call(functools.partial(pack_kernel, half=half), out_shape=jax.S...  1.93 us
    another operation x1, other arithmetic  1.17 us
  transfers between devices with their start and end apart: 11, of which 9 were waited for; matrix products, arithmetic and copies ran while one was open for 0% of the time, Pallas kernels for 0%

profile of v1, /device:TPU:0, one launch (start us, length us, event | category | flops | bytes accessed | tf_op | source)
XLA Modules:
  0.0 56.2 jit_solution(15277109575101789859)
XLA Ops:
  0.0 1.4 %copy.9.route_ref = s32[64,4]{1,0:T(8,128)} copy(s32[64,4]{0,1:T(4,128)} %param.9) | data formatting | bytes 2048 | tf_op args[1]
  1.4 1.4 %copy.10.weight_ref = f32[64,4]{1,0:T(8,128)} copy(f32[64,4]{0,1:T(4,128)} %param.10) | data formatting | bytes 2048 | tf_op args[2]
  2.8 1.9 %pack.1.refs_0_ = bf16[64,2176]{1,0:T(8,128)(2,1)} custom-call(bf16[64,2048]{1,0:T(8,128)(2,1)} %tok_ref.1, s32[64,4]{1,0:T(8,128)} %copy.9.route_ref, f32[64,4]{1,0:T(8,128)} %copy.10.weight_ref, f32[1,2048]{1,0:T(1,128)} %bitcast.15), custom_call_target="tpu_custom_call" | custom-call | tf_op jit(solution)/shard_map/pack/pallas_call | solution.py:33
  4.7 3.0 %collective-permute-start.1 = (bf16[64,2176]{1,0:T(8,128)(2,1)}, bf16[64,2176]{1,0:T(8,128)(2,1)S(1)}, u32[]{:S(2)}, u32[]{:S(2)}) collective-permute-start(bf16[64,2176]{1,0:T(8,128)(2,1)} %pack.1.refs_0_), channel_id=1, source_target_pairs={{0,8},{4,12},{8,0},{12,4},{1,9},{5,13},{9,1},{13,5},{2,10},{6,14},... | collective-permute-start | bytes 835592 | tf_op jit(solution)/shard_map/ppermute | solution.py:110
  7.7 0.0 collective-permute-start
  7.7 6.9 %collective-permute-done.1.refs_2_ = bf16[64,2176]{1,0:T(8,128)(2,1)S(1)} collective-permute-done((bf16[64,2176]{1,0:T(8,128)(2,1)}, bf16[64,2176]{1,0:T(8,128)(2,1)S(1)}, u32[]{:S(2)}, u32[]{:S(2)}) %collective-permute-start.1) | collective-permute-done | bytes 278560 | tf_op jit(solution)/shard_map/ppermute | solution.py:110
  14.6 0.0 copy-start
  14.6 0.0 collective-permute-start.2
  14.6 0.0 collective-permute-done.refs_1_
  14.6 0.0 copy-start.1
  14.6 1.5 %collective-permute-done.2.refs_3_ = bf16[64,2176]{1,0:T(8,128)(2,1)S(1)} collective-permute-done((bf16[64,2176]{1,0:T(8,128)(2,1)S(1)}, bf16[64,2176]{1,0:T(8,128)(2,1)S(1)}, u32[]{:S(2)}, u32[]{:S(2)}) %collective-permute-start.2) | collective-permute-done | bytes 278560 | tf_op jit(solution)/shard_map/ppermute | solution.py:110
  16.1 0.0 copy-start.2
  16.1 0.0 copy-done
  16.1 0.0 copy-done.1
  16.1 0.7 %copy-done.2 = bf16[64,2176]{1,0:T(8,128)(2,1)} copy-done((bf16[64,2176]{1,0:T(8,128)(2,1)}, bf16[64,2176]{1,0:T(8,128)(2,1)S(1)}, u32[]{:S(2)}) %copy-start.2) | copy-done | bytes 278552
  16.8 0.0 copy-start.3
  16.9 9.5 %experts.1 = (bf16[2,64,2048]{2,1,0:T(8,128)(2,1)}, bf16[2,64,2048]{2,1,0:T(8,128)(2,1)}) custom-call(s32[1]{0:T(128)} %bitcast.place_ref, bf16[64,2176]{1,0:T(8,128)(2,1)} %pack.1.refs_0_, bf16[64,2176]{1,0:T(8,128)(2,1)} %copy-done.1, bf16[64,2176]{1,0:T(8,128)(2,1)} %copy-done, bf16[64,2176]{1,0:T(8,128)(2,1)} %copy-done.2, ...), custom_call_target="tpu_custom_call" | custom-call | tf_op jit(solution)/shard_map/experts/pallas_call | solution.py:86
  26.3 0.1 collective-permute-start.3
  26.5 2.0 %collective-permute-done.3 = bf16[2,64,2048]{2,1,0:T(8,128)(2,1)S(1)} collective-permute-done((bf16[2,64,2048]{2,1,0:T(8,128)(2,1)}, bf16[2,64,2048]{2,1,0:T(8,128)(2,1)S(1)}, u32[]{:S(2)}, u32[]{:S(2)}) %collective-permute-start.3) | collective-permute-done | bytes 524320 | tf_op jit(solution)/shard_map/ppermute | solution.py:110
  28.5 1.2 %add_convert_fusion = bf16[2,64,2048]{2,1,0:T(8,128)(2,1)S(1)} fusion(bf16[2,64,2048]{2,1,0:T(8,128)(2,1)S(1)} %collective-permute-done.3, bf16[2,64,2048]{2,1,0:T(8,128)(2,1)} %get-tuple-element.7), kind=kLoop, calls=%fused_computation | loop fusion | flops 1048576 | bytes 1572864 | tf_op jit(solution)/shard_map/convert.2
  29.7 1.8 %collective-permute-start.4 = (bf16[1,64,2048]{2,1,0:T(8,128)(2,1)S(1)}, bf16[1,64,2048]{2,1,0:T(8,128)(2,1)S(1)}, u32[]{:S(2)}, u32[]{:S(2)}) collective-permute-start(bf16[1,64,2048]{2,1,0:T(8,128)(2,1)S(1)} %slice.13), channel_id=1, source_target_pairs={{0,8},{4,12},{8,0},{12,4},{1,9},{5,13},{9,1},{13,5},{2,10},{6,14},... | collective-permute-start | bytes 786440 | tf_op jit(solution)/shard_map/ppermute | solution.py:110
  31.5 6.6 %collective-permute-done.4 = bf16[1,64,2048]{2,1,0:T(8,128)(2,1)S(1)} collective-permute-done((bf16[1,64,2048]{2,1,0:T(8,128)(2,1)S(1)}, bf16[1,64,2048]{2,1,0:T(8,128)(2,1)S(1)}, u32[]{:S(2)}, u32[]{:S(2)}) %collective-permute-start.4) | collective-permute-done | bytes 262176 | tf_op jit(solution)/shard_map/ppermute | solution.py:110
  38.1 0.1 add_convert_fusion.1
  38.2 3.9 %collective-permute-start.7 = (bf16[64,512]{1,0:T(8,128)(2,1)S(1)}, bf16[64,512]{1,0:T(8,128)(2,1)S(1)}, u32[]{:S(2)}, u32[]{:S(2)}) collective-permute-start(bf16[64,512]{1,0:T(8,128)(2,1)S(1)} %get-tuple-element.10), channel_id=1, source_target_pairs={{0,3},{1,0},{2,1},{3,2},{4,7},{5,4},{6,5},{7,6},{8,11},{9,8},{10,9... | collective-permute-start | bytes 196616 | tf_op jit(solution)/shard_map/ppermute | solution.py:114
  42.1 0.0 collective-permute-start.6
  42.1 1.0 %collective-permute-start.5 = (bf16[64,512]{1,0:T(8,128)(2,1)S(1)}, bf16[64,512]{1,0:T(8,128)(2,1)S(1)}, u32[]{:S(2)}, u32[]{:S(2)}) collective-permute-start(bf16[64,512]{1,0:T(8,128)(2,1)S(1)} %get-tuple-element.9), channel_id=1, source_target_pairs={{0,1},{1,2},{2,3},{3,0},{4,5},{5,6},{6,7},{7,4},{8,9},{9,10},{10,1... | collective-permute-start | bytes 196616 | tf_op jit(solution)/shard_map/ppermute | solution.py:114
  43.1 1.2 %collective-permute-done.7 = bf16[64,512]{1,0:T(8,128)(2,1)S(1)} collective-permute-done((bf16[64,512]{1,0:T(8,128)(2,1)S(1)}, bf16[64,512]{1,0:T(8,128)(2,1)S(1)}, u32[]{:S(2)}, u32[]{:S(2)}) %collective-permute-start.7) | collective-permute-done | bytes 65568 | tf_op jit(solution)/shard_map/ppermute | solution.py:114
  44.3 3.1 %collective-permute-done.6 = bf16[64,512]{1,0:T(8,128)(2,1)S(1)} collective-permute-done((bf16[64,512]{1,0:T(8,128)(2,1)S(1)}, bf16[64,512]{1,0:T(8,128)(2,1)S(1)}, u32[]{:S(2)}, u32[]{:S(2)}) %collective-permute-start.6) | collective-permute-done | bytes 65568 | tf_op jit(solution)/shard_map/ppermute | solution.py:114
  47.4 0.8 %collective-permute-done.5 = bf16[64,512]{1,0:T(8,128)(2,1)S(1)} collective-permute-done((bf16[64,512]{1,0:T(8,128)(2,1)S(1)}, bf16[64,512]{1,0:T(8,128)(2,1)S(1)}, u32[]{:S(2)}, u32[]{:S(2)}) %collective-permute-start.5) | collective-permute-done | bytes 65568 | tf_op jit(solution)/shard_map/ppermute | solution.py:114
  48.1 0.1 multiply_reduce_fusion
  48.3 1.8 %collective-permute-start.10 = (f32[64]{0:T(128)S(1)}, f32[64]{0:T(128)S(1)}, u32[]{:S(2)}, u32[]{:S(2)}) collective-permute-start(f32[64]{0:T(128)S(1)} %multiply_reduce_fusion), channel_id=1, source_target_pairs={{0,3},{1,0},{2,1},{3,2},{4,7},{5,4},{6,5},{7,6},{8,11},{9,8},{10,9... | collective-permute-start | bytes 776 | tf_op jit(solution)/shard_map/ppermute | solution.py:114
  50.1 0.0 collective-permute-start.9
  50.1 1.9 %collective-permute-start.8 = (f32[64]{0:T(128)S(1)}, f32[64]{0:T(128)S(1)}, u32[]{:S(2)}, u32[]{:S(2)}) collective-permute-start(f32[64]{0:T(128)S(1)} %multiply_reduce_fusion), channel_id=1, source_target_pairs={{0,1},{1,2},{2,3},{3,0},{4,5},{5,6},{6,7},{7,4},{8,9},{9,10},{10,1... | collective-permute-start | bytes 776 | tf_op jit(solution)/shard_map/ppermute | solution.py:114
  52.0 0.0 collective-permute-done.10
  52.0 2.6 %collective-permute-done.9 = f32[64]{0:T(128)S(1)} collective-permute-done((f32[64]{0:T(128)S(1)}, f32[64]{0:T(128)S(1)}, u32[]{:S(2)}, u32[]{:S(2)}) %collective-permute-start.9) | collective-permute-done | bytes 288 | tf_op jit(solution)/shard_map/ppermute | solution.py:114
  54.5 0.9 %collective-permute-done.8 = f32[64]{0:T(128)S(1)} collective-permute-done((f32[64]{0:T(128)S(1)}, f32[64]{0:T(128)S(1)}, u32[]{:S(2)}, u32[]{:S(2)}) %collective-permute-start.8) | collective-permute-done | bytes 288 | tf_op jit(solution)/shard_map/ppermute | solution.py:114
  55.4 0.0 copy-done.3
  55.5 0.7 %multiply_convert_fusion = bf16[64,512]{1,0:T(8,128)(2,1)} fusion(f32[512]{0:T(512)S(1)} %copy-done.3, f32[64]{0:T(128)S(1)} %add_rsqrt_fusion, bf16[64,512]{1,0:T(8,128)(2,1)S(1)} %collective-permute-done.7, bf16[64,512]{1,0:T(8,128)(2,1)S(1)} %collective-permute-done.6, bf16[64,512]{1,0:T(8,128)(2,1)S(1)} %collective-permute-done.5, ...), kind=kLoop, calls=%fused_computation.5 | loop fusion | flops 327680 | bytes 329988 | tf_op jit(solution)/shard_map/convert_element_type | solution.py:156
  (3 shorter events, 0.1 us)
Async XLA Ops:
  4.7 9.9 %collective-permute-start.1 = (bf16[64,2176]{1,0:T(8,128)(2,1)}, bf16[64,2176]{1,0:T(8,128)(2,1)S(1)}, u32[]{:S(2)}, u32[]{:S(2)}) collective-permute-start(bf16[64,2176]{1,0:T(8,128)(2,1)} %pack.1.refs_0_), channel_id=1, source_target_pairs={{0,8},{4,12},{8,0},{12,4},{1,9},{5,13},{9,1},{13,5},{2,10},{6,14},... | collective-permute-start | bytes 835592 | tf_op jit(solution)/shard_map/ppermute | solution.py:110
  7.7 6.9 %collective-permute-start = (bf16[64,2176]{1,0:T(8,128)(2,1)}, bf16[64,2176]{1,0:T(8,128)(2,1)S(1)}, u32[]{:S(2)}, u32[]{:S(2)}) collective-permute-start(bf16[64,2176]{1,0:T(8,128)(2,1)} %pack.1.refs_0_), channel_id=1, source_target_pairs={{0,4},{4,0},{8,12},{12,8},{1,5},{5,1},{9,13},{13,9},{2,6},{6,2},{1... | collective-permute-start | bytes 835592 | tf_op jit(solution)/shard_map/ppermute | solution.py:110
  14.6 1.6 %copy-start = (bf16[64,2176]{1,0:T(8,128)(2,1)}, bf16[64,2176]{1,0:T(8,128)(2,1)S(1)}, u32[]{:S(2)}) copy-start(bf16[64,2176]{1,0:T(8,128)(2,1)S(1)} %collective-permute-done.1.refs_2_) | copy-start | bytes 835588
  14.6 1.6 %collective-permute-start.2 = (bf16[64,2176]{1,0:T(8,128)(2,1)S(1)}, bf16[64,2176]{1,0:T(8,128)(2,1)S(1)}, u32[]{:S(2)}, u32[]{:S(2)}) collective-permute-start(bf16[64,2176]{1,0:T(8,128)(2,1)S(1)} %collective-permute-done.1.refs_2_), channel_id=1, source_target_pairs={{0,4},{4,0},{8,12},{12,8},{1,5},{5,1},{9,13},{13,9},{2,6},{6,2},{1... | collective-permute-start | bytes 835592 | tf_op jit(solution)/shard_map/ppermute | solution.py:110
  14.6 1.6 %copy-start.1 = (bf16[64,2176]{1,0:T(8,128)(2,1)}, bf16[64,2176]{1,0:T(8,128)(2,1)S(1)}, u32[]{:S(2)}) copy-start(bf16[64,2176]{1,0:T(8,128)(2,1)S(1)} %collective-permute-done.refs_1_) | copy-start | bytes 835588
  16.1 0.7 %copy-start.2 = (bf16[64,2176]{1,0:T(8,128)(2,1)}, bf16[64,2176]{1,0:T(8,128)(2,1)S(1)}, u32[]{:S(2)}) copy-start(bf16[64,2176]{1,0:T(8,128)(2,1)S(1)} %collective-permute-done.2.refs_3_) | copy-start | bytes 835588
  16.8 38.6 %copy-start.3 = (f32[512]{0:T(512)S(1)}, f32[512]{0:T(512)}, u32[]{:S(2)}) copy-start(f32[512]{0:T(512)} %param.15) | copy-start | bytes 6148
  26.3 2.1 %collective-permute-start.3 = (bf16[2,64,2048]{2,1,0:T(8,128)(2,1)}, bf16[2,64,2048]{2,1,0:T(8,128)(2,1)S(1)}, u32[]{:S(2)}, u32[]{:S(2)}) collective-permute-start(bf16[2,64,2048]{2,1,0:T(8,128)(2,1)} %get-tuple-element.8), channel_id=1, source_target_pairs={{0,4},{4,0},{8,12},{12,8},{1,5},{5,1},{9,13},{13,9},{2,6},{6,2},{1... | collective-permute-start | bytes 1572872 | tf_op jit(solution)/shard_map/ppermute | solution.py:110
  29.7 8.4 %collective-permute-start.4 = (bf16[1,64,2048]{2,1,0:T(8,128)(2,1)S(1)}, bf16[1,64,2048]{2,1,0:T(8,128)(2,1)S(1)}, u32[]{:S(2)}, u32[]{:S(2)}) collective-permute-start(bf16[1,64,2048]{2,1,0:T(8,128)(2,1)S(1)} %slice.13), channel_id=1, source_target_pairs={{0,8},{4,12},{8,0},{12,4},{1,9},{5,13},{9,1},{13,5},{2,10},{6,14},... | collective-permute-start | bytes 786440 | tf_op jit(solution)/shard_map/ppermute | solution.py:110
  38.2 6.1 %collective-permute-start.7 = (bf16[64,512]{1,0:T(8,128)(2,1)S(1)}, bf16[64,512]{1,0:T(8,128)(2,1)S(1)}, u32[]{:S(2)}, u32[]{:S(2)}) collective-permute-start(bf16[64,512]{1,0:T(8,128)(2,1)S(1)} %get-tuple-element.10), channel_id=1, source_target_pairs={{0,3},{1,0},{2,1},{3,2},{4,7},{5,4},{6,5},{7,6},{8,11},{9,8},{10,9... | collective-permute-start | bytes 196616 | tf_op jit(solution)/shard_map/ppermute | solution.py:114
  42.1 5.3 %collective-permute-start.6 = (bf16[64,512]{1,0:T(8,128)(2,1)S(1)}, bf16[64,512]{1,0:T(8,128)(2,1)S(1)}, u32[]{:S(2)}, u32[]{:S(2)}) collective-permute-start(bf16[64,512]{1,0:T(8,128)(2,1)S(1)} %get-tuple-element.11), channel_id=1, source_target_pairs={{0,2},{1,3},{2,0},{3,1},{4,6},{5,7},{6,4},{7,5},{8,10},{9,11},{10,... | collective-permute-start | bytes 196616 | tf_op jit(solution)/shard_map/ppermute | solution.py:114
  42.1 6.1 %collective-permute-start.5 = (bf16[64,512]{1,0:T(8,128)(2,1)S(1)}, bf16[64,512]{1,0:T(8,128)(2,1)S(1)}, u32[]{:S(2)}, u32[]{:S(2)}) collective-permute-start(bf16[64,512]{1,0:T(8,128)(2,1)S(1)} %get-tuple-element.9), channel_id=1, source_target_pairs={{0,1},{1,2},{2,3},{3,0},{4,5},{5,6},{6,7},{7,4},{8,9},{9,10},{10,1... | collective-permute-start | bytes 196616 | tf_op jit(solution)/shard_map/ppermute | solution.py:114
  48.3 3.7 %collective-permute-start.10 = (f32[64]{0:T(128)S(1)}, f32[64]{0:T(128)S(1)}, u32[]{:S(2)}, u32[]{:S(2)}) collective-permute-start(f32[64]{0:T(128)S(1)} %multiply_reduce_fusion), channel_id=1, source_target_pairs={{0,3},{1,0},{2,1},{3,2},{4,7},{5,4},{6,5},{7,6},{8,11},{9,8},{10,9... | collective-permute-start | bytes 776 | tf_op jit(solution)/shard_map/ppermute | solution.py:114
  50.1 4.5 %collective-permute-start.9 = (f32[64]{0:T(128)S(1)}, f32[64]{0:T(128)S(1)}, u32[]{:S(2)}, u32[]{:S(2)}) collective-permute-start(f32[64]{0:T(128)S(1)} %multiply_reduce_fusion), channel_id=1, source_target_pairs={{0,2},{1,3},{2,0},{3,1},{4,6},{5,7},{6,4},{7,5},{8,10},{9,11},{10,... | collective-permute-start | bytes 776 | tf_op jit(solution)/shard_map/ppermute | solution.py:114
  50.1 5.4 %collective-permute-start.8 = (f32[64]{0:T(128)S(1)}, f32[64]{0:T(128)S(1)}, u32[]{:S(2)}, u32[]{:S(2)}) collective-permute-start(f32[64]{0:T(128)S(1)} %multiply_reduce_fusion), channel_id=1, source_target_pairs={{0,1},{1,2},{2,3},{3,0},{4,5},{5,6},{6,7},{7,4},{8,9},{9,10},{10,1... | collective-permute-start | bytes 776 | tf_op jit(solution)/shard_map/ppermute | solution.py:114

commit v2 on v1

v2 whole, which is shorter than its diff:
```python
import functools

import jax
import jax.numpy as jnp
from jax import lax
from jax.experimental import pallas as pl
from jax.experimental.pallas import tpu as pltpu
from jax.sharding import PartitionSpec as P


LIMIT = 7.0
ALPHA = 1.702
EPS = 1e-06


def pack_kernel(tok_ref, route_ref, weight_ref, gain_ref, out_ref, *, half):
    width = tok_ref.shape[1]
    scaled = tok_ref[...].astype(jnp.float32)
    mean = jnp.mean(scaled * scaled, axis=-1, keepdims=True)
    out_ref[:, :width] = (scaled * lax.rsqrt(mean + EPS) * gain_ref[...]).astype(jnp.bfloat16)
    rows = tok_ref.shape[0]
    line = lax.broadcasted_iota(jnp.int32, (2 * half, rows), 0)
    expert = jnp.where(line < half, line, line - half)
    dense = jnp.zeros((2 * half, rows), jnp.float32)
    for k in range(route_ref.shape[0]):
        dense += jnp.where(route_ref[k : k + 1, :] == expert, weight_ref[k : k + 1, :], 0.0)
    high = dense.astype(jnp.bfloat16).astype(jnp.float32)
    split = jnp.where(line < half, high, dense - high)
    out_ref[:, width:] = split.T.astype(jnp.bfloat16)


def pack(tokens, routing, route_weight, norm_gain, half):
    rows, width = tokens.shape
    return pl.pallas_call(
        functools.partial(pack_kernel, half=half),
        out_shape=jax.ShapeDtypeStruct((rows, width + 2 * half), jnp.bfloat16),
        compiler_params=pltpu.CompilerParams(vmem_limit_bytes=16 * 2**20),
        name="pack",
    )(tokens, routing.T, route_weight.T, norm_gain.reshape(1, width))


def moe_kernel(place_ref, *refs, blocks, half, chunk):
    x_refs = refs[:blocks]
    gate_ref, up_ref, down_ref, keep_ref, send_ref, x_all, w_all, acc = refs[blocks:]
    rows = x_refs[0].shape[0]
    width = x_all.shape[1]
    for b in range(blocks):
        x_all[b * rows : (b + 1) * rows, :] = x_refs[b][:, :width]
        w_all[b * rows : (b + 1) * rows, :] = x_refs[b][:, width:].astype(jnp.float32)
    lane = lax.broadcasted_iota(jnp.int32, w_all.shape, 1)
    for e in range(gate_ref.shape[0]):
        expert = place_ref[0] + e
        mine = (lane == expert) | (lane == expert + half)
        weight = jnp.sum(jnp.where(mine, w_all[...], 0.0), axis=1, keepdims=True)
        for c in range(0, gate_ref.shape[2], chunk):
            x = x_all[...]
            gate = jnp.dot(x, gate_ref[e, :, c : c + chunk], preferred_element_type=jnp.float32)
            up = jnp.dot(x, up_ref[e, :, c : c + chunk], preferred_element_type=jnp.float32)
            gate = jnp.minimum(gate, LIMIT)
            up = jnp.clip(up, -LIMIT, LIMIT)
            hidden = (up + 1.0) * gate * jax.nn.sigmoid(ALPHA * gate) * weight
            part = jnp.dot(
                hidden.astype(jnp.bfloat16), down_ref[e, c : c + chunk, :],
                preferred_element_type=jnp.float32,
            )
            if e == 0 and c == 0:
                acc[...] = part
            else:
                acc[...] += part
    for b in range(blocks // 2):
        keep_ref[b] = acc[2 * b * rows : (2 * b + 1) * rows, :].astype(jnp.bfloat16)
        send_ref[b] = acc[(2 * b + 1) * rows : (2 * b + 2) * rows, :].astype(jnp.bfloat16)


def fetch_kernel(*refs):
    count = (len(refs) - 2) // 2
    sources, targets, sems = refs[1 : 1 + count], refs[1 + count : -1], refs[-1]
    copies = [pltpu.make_async_copy(a, b, sems.at[i]) for i, (a, b) in enumerate(zip(sources, targets))]
    for copy in copies:
        copy.start()
    for copy in copies:
        copy.wait()


def fetch(after, weights):
    size = sum(w.size for w in weights)
    return pl.pallas_call(
        fetch_kernel,
        in_specs=[pl.BlockSpec(memory_space=pl.ANY)] * (1 + len(weights)),
        out_specs=[pl.BlockSpec(memory_space=pltpu.VMEM)] * len(weights),
        out_shape=[pltpu.VMEM(w.shape, w.dtype) for w in weights],
        scratch_shapes=[pltpu.SemaphoreType.DMA((len(weights),))],
        compiler_params=pltpu.CompilerParams(vmem_limit_bytes=16 * 2**20),
        cost_estimate=pl.CostEstimate(flops=256 * size, bytes_accessed=4 * size, transcendentals=0),
        name="fetch",
    )(after, *[pltpu.with_memory_space_constraint(w, pltpu.HBM) for w in weights])


def run_experts(x_blocks, gate_weight, up_weight, down_weight, place, half):
    blocks = len(x_blocks)
    rows = x_blocks[0].shape[0]
    width, hidden = gate_weight.shape[1:]
    out = jax.ShapeDtypeStruct((blocks // 2, rows, width), jnp.bfloat16)
    return pl.pallas_call(
        functools.partial(moe_kernel, blocks=blocks, half=half, chunk=min(hidden, 256)),
        in_specs=[pl.BlockSpec(memory_space=pltpu.SMEM)]
        + [pl.BlockSpec(memory_space=pltpu.VMEM)] * (blocks + 3),
        scratch_shapes=[
            pltpu.VMEM((blocks * rows, width), jnp.bfloat16),
            pltpu.VMEM((blocks * rows, 2 * half), jnp.float32),
            pltpu.VMEM((blocks * rows, width), jnp.float32),
        ],
        out_shape=[out, out],
        compiler_params=pltpu.CompilerParams(vmem_limit_bytes=40 * 2**20),
        name="experts",
    )(place, *x_blocks, *[pltpu.with_memory_space_constraint(w, pltpu.VMEM) for w in (gate_weight, up_weight, down_weight)])


def swap(value, axis, size, bit):
    return lax.ppermute(value, axis, [(s, s ^ bit) for s in range(size)])


def shift(value, axis, size, amount):
    return lax.ppermute(value, axis, [(s, (s + amount) % size) for s in range(size)])


def on_device(
    ep_size, tp_size,
    tokens, routing, route_weight, norm_gain, gate_weight, up_weight, down_weight, out_gain
):
    model_width = tokens.shape[1]
    local_experts = gate_weight.shape[0]
    all_experts = local_experts * ep_size
    half = -(-all_experts // 64) * 64
    ep_index = lax.axis_index("ep")
    tp_index = lax.axis_index("tp")
    bits = [1 << b for b in range(ep_size.bit_length() - 1)]

    place = (ep_index * local_experts).astype(jnp.int32).reshape(1)
    place, tokens = lax.optimization_barrier((place, tokens))
    packed = pack(tokens, routing, route_weight, norm_gain, half)
    weights = fetch(packed, (gate_weight, up_weight, down_weight))
    arrived = {0: packed, bits[-1]: swap(packed, "ep", ep_size, bits[-1])}
    for bit in reversed(bits[:-1]):
        for j in list(arrived):
            arrived[j ^ bit] = swap(arrived[j], "ep", ep_size, bit)
    x_blocks = [arrived[j] for j in range(ep_size)]
    keep, send = run_experts(x_blocks, *weights, place, half)
    for bit in bits:
        got = swap(send, "ep", ep_size, bit)
        total = keep.astype(jnp.float32) + got.astype(jnp.float32)
        if bit == bits[-1]:
            mixed = total[0].astype(jnp.bfloat16)
        else:
            keep = total[0::2].astype(jnp.bfloat16)
            send = total[1::2].astype(jnp.bfloat16)
    out_width = model_width // tp_size
    block = lambda d: lax.dynamic_slice_in_dim(
        mixed, ((tp_index + d) % tp_size) * out_width, out_width, axis=1
    )
    expert_mix = block(0).astype(jnp.float32)
    for d in range(1, tp_size):
        expert_mix += shift(block(d), "tp", tp_size, d).astype(jnp.float32)
    square = jnp.sum(expert_mix * expert_mix, axis=1)
    copies = jnp.broadcast_to(square, (tp_size,) + square.shape)
    square_sum = jnp.sum(lax.all_to_all(copies, "tp", 0, 0, tiled=True), axis=0)
    scale_factor = lax.rsqrt(square_sum / model_width + EPS)
    return (expert_mix * scale_factor[:, None] * out_gain).astype(jnp.bfloat16)


def solution(mesh):
    in_specs = (
        P(("grp", "ep"), None),
        P(("grp", "ep"), None),
        P(("grp", "ep"), None),
        P(),
        P("ep", None, "tp"),
        P("ep", None, "tp"),
        P("ep", "tp", None),
        P("tp"),
    )
    out_specs = P(("grp", "ep"), "tp")
    return jax.shard_map(
        functools.partial(on_device, mesh.shape["ep"], mesh.shape["tp"]),
        mesh=mesh, in_specs=in_specs, out_specs=out_specs, check_vma=False
    )
```

time: 56.4 us -> 53.2 us (0.943)
  blocking collectives: 0 us -> 9.44 us
  waiting for transfers between devices: 25.5 us -> 18.5 us
  starting transfers between devices: 13.5 us -> 11.2 us
  Pallas kernels: 11.4 us -> 9.55 us
  other arithmetic: 2.09 us -> 1.07 us
    all_to_all x0 -> x1, blocking collectives: none -> 9.44 us  [on_device(): square_sum = jnp.sum(lax.all_to_all(copies, 'tp', 0, 0, tiled=True), axis=0)]
    ppermute x6 -> x3, waiting for transfers between devices: 8.53 us -> 3.28 us  [shift(): lax.ppermute(value, axis, [(s, (s + amount) % size) for s in range(size)])]
    pallas_call x1, Pallas kernels: 9.49 us -> 4.71 us  [run_experts(): pl.pallas_call(functools.partial(moe_kernel, blocks=blocks, half=half, ch...]
    pallas_call x0 -> x1, Pallas kernels: none -> 4.69 us  [fetch(): pl.pallas_call(fetch_kernel, in_specs=[pl.BlockSpec(memory_space=pl.ANY)]...]
    ppermute x6 -> x3, starting transfers between devices: 8.58 us -> 5.79 us  [shift(): lax.ppermute(value, axis, [(s, (s + amount) % size) for s in range(size)])]
    pallas_call x1, Pallas kernels: 1.93 us -> 0.16 us  [pack(): pl.pallas_call(functools.partial(pack_kernel, half=half), out_shape=jax.S...]
    ppermute x5, waiting for transfers between devices: 17 us -> 15.3 us  [swap(): return lax.ppermute(value, axis, [(s, s ^ bit) for s in range(size)])]
    another operation x1, other arithmetic: 1.17 us -> 0.12 us
  transfers between devices with their start and end apart: 11 -> 8, of which waited for: 9 -> 5; matrix products, arithmetic and copies ran while one was open for 0% -> 0% of each run, Pallas kernels for 0% -> 9%
where the time goes in v2:
time: 53.2 us; the launch traced here: 52.9 us
  waiting for transfers between devices  18.5 us (35%)
  starting transfers between devices  11.2 us (21%)
  Pallas kernels  9.55 us (18%)
  blocking collectives  9.44 us (18%)
  local copies, waits for them, and re-layouts  3.06 us (6%)
  other arithmetic  1.07 us (2%)
    ppermute x5, waiting for transfers between devices, swap(): return lax.ppermute(value, axis, [(s, s ^ bit) for s in range(size)])  15.3 us
    all_to_all x1, blocking collectives, on_device(): square_sum = jnp.sum(lax.all_to_all(copies, 'tp', 0, 0, tiled=True), axis=0)  9.44 us
    ppermute x3, starting transfers between devices, shift(): lax.ppermute(value, axis, [(s, (s + amount) % size) for s in range(size)])  5.79 us
    ppermute x5, starting transfers between devices, swap(): return lax.ppermute(value, axis, [(s, s ^ bit) for s in range(size)])  5.36 us
    pallas_call x1, Pallas kernels, run_experts(): pl.pallas_call(functools.partial(moe_kernel, blocks=blocks, half=half, ch...  4.71 us
    pallas_call x1, Pallas kernels, fetch(): pl.pallas_call(fetch_kernel, in_specs=[pl.BlockSpec(memory_space=pl.ANY)]...  4.69 us
    ppermute x3, waiting for transfers between devices, shift(): lax.ppermute(value, axis, [(s, (s + amount) % size) for s in range(size)])  3.28 us
    unnamed x10, local copies, waits for them, and re-layouts  3.01 us
  transfers between devices with their start and end apart: 8, of which 5 were waited for; matrix products, arithmetic and copies ran while one was open for 0% of the time, Pallas kernels for 9%

profile of v2, /device:TPU:0, one launch (start us, length us, event | category | flops | bytes accessed | tf_op | source)
XLA Modules:
  0.0 52.9 jit_solution(7665252049621310842)
XLA Ops:
  0.0 0.0 copy-start
  0.0 0.9 %copy-done = bf16[64,2048]{1,0:T(8,128)(2,1)S(1)} copy-done((bf16[64,2048]{1,0:T(8,128)(2,1)S(1)}, bf16[64,2048]{1,0:T(8,128)(2,1)}, u32[]{:S(2)}) %copy-start) | copy-done | bytes 262168
  1.0 0.0 copy-start.1
  1.0 0.7 %copy-done.1 = f32[2048]{0:T(1024)S(1)} copy-done((f32[2048]{0:T(1024)S(1)}, f32[2048]{0:T(1024)}, u32[]{:S(2)}) %copy-start.1) | copy-done | bytes 8216
  1.6 0.0 copy-start.2
  1.7 0.7 %copy-done.2 = s32[64,4]{0,1:T(4,128)S(1)} copy-done((s32[64,4]{0,1:T(4,128)S(1)}, s32[64,4]{0,1:T(4,128)}, u32[]{:S(2)}) %copy-start.2) | copy-done | bytes 1048
  2.3 0.0 copy-start.3
  2.3 0.7 %copy-done.3 = f32[64,4]{0,1:T(4,128)S(1)} copy-done((f32[64,4]{0,1:T(4,128)S(1)}, f32[64,4]{0,1:T(4,128)}, u32[]{:S(2)}) %copy-start.3) | copy-done | bytes 1048
  3.0 0.2 pack.1.refs_0_
  3.2 3.1 %collective-permute-start.1 = (bf16[64,2176]{1,0:T(8,128)(2,1)S(1)}, bf16[64,2176]{1,0:T(8,128)(2,1)S(1)}, u32[]{:S(2)}, u32[]{:S(2)}) collective-permute-start(bf16[64,2176]{1,0:T(8,128)(2,1)S(1)} %pack.1.refs_0_), channel_id=1, source_target_pairs={{0,8},{4,12},{8,0},{12,4},{1,9},{5,13},{9,1},{13,5},{2,10},{6,14},... | collective-permute-start | bytes 835592 | tf_op jit(solution)/shard_map/ppermute | solution.py:120
  6.2 0.0 collective-permute-start
  6.2 6.7 %collective-permute-done.1.refs_2_ = bf16[64,2176]{1,0:T(8,128)(2,1)S(1)} collective-permute-done((bf16[64,2176]{1,0:T(8,128)(2,1)S(1)}, bf16[64,2176]{1,0:T(8,128)(2,1)S(1)}, u32[]{:S(2)}, u32[]{:S(2)}) %collective-permute-start.1) | collective-permute-done | bytes 278560 | tf_op jit(solution)/shard_map/ppermute | solution.py:120
  12.9 0.0 collective-permute-start.2
  12.9 4.7 %fetch.1 = (bf16[2,2048,512]{2,1,0:T(8,128)(2,1)S(1)}, bf16[2,2048,512]{2,1,0:T(8,128)(2,1)S(1)}, bf16[2,512,2048]{2,1,0:T(8,128)(2,1)S(1)}) custom-call(bf16[64,2176]{1,0:T(8,128)(2,1)S(1)} %pack.1.refs_0_, bf16[2,2048,512]{2,1,0:T(8,128)(2,1)} %refs_1_.1, bf16[2,2048,512]{2,1,0:T(8,128)(2,1)} %refs_2_.1, bf16[2,512,2048]{2,1,0:T(8,128)(2,1)} %refs_3_.1), custom_call_target="tpu_custom_call" | custom-call | flops 1610612736 | bytes 25165824 | tf_op jit(solution)/shard_map/fetch/pallas_call | solution.py:87
  17.6 0.0 collective-permute-done.refs_1_
  17.6 0.0 collective-permute-done.2.refs_3_
  17.6 0.0 copy-start.4
  17.6 4.7 %experts.1 = (bf16[2,64,2048]{2,1,0:T(8,128)(2,1)S(1)}, bf16[2,64,2048]{2,1,0:T(8,128)(2,1)}) custom-call(s32[1]{0:T(128)} %bitcast.place_ref, bf16[64,2176]{1,0:T(8,128)(2,1)S(1)} %pack.1.refs_0_, bf16[64,2176]{1,0:T(8,128)(2,1)S(1)} %collective-permute-done.refs_1_, bf16[64,2176]{1,0:T(8,128)(2,1)S(1)} %collective-permute-done.1.refs_2_, ...), custom_call_target="tpu_custom_call" | custom-call | tf_op jit(solution)/shard_map/experts/pallas_call | solution.py:104
  22.3 0.5 collective-permute-start.3
  22.8 1.7 %collective-permute-done.3 = bf16[2,64,2048]{2,1,0:T(8,128)(2,1)S(1)} collective-permute-done((bf16[2,64,2048]{2,1,0:T(8,128)(2,1)}, bf16[2,64,2048]{2,1,0:T(8,128)(2,1)S(1)}, u32[]{:S(2)}, u32[]{:S(2)}) %collective-permute-start.3) | collective-permute-done | bytes 524320 | tf_op jit(solution)/shard_map/ppermute | solution.py:120
  24.6 0.1 add_convert_fusion
  24.7 1.8 %collective-permute-start.4 = (bf16[1,64,2048]{2,1,0:T(8,128)(2,1)S(1)}, bf16[1,64,2048]{2,1,0:T(8,128)(2,1)S(1)}, u32[]{:S(2)}, u32[]{:S(2)}) collective-permute-start(bf16[1,64,2048]{2,1,0:T(8,128)(2,1)S(1)} %slice.13), channel_id=1, source_target_pairs={{0,8},{4,12},{8,0},{12,4},{1,9},{5,13},{9,1},{13,5},{2,10},{6,14},... | collective-permute-start | bytes 786440 | tf_op jit(solution)/shard_map/ppermute | solution.py:120
  26.5 6.8 %collective-permute-done.4 = bf16[1,64,2048]{2,1,0:T(8,128)(2,1)S(1)} collective-permute-done((bf16[1,64,2048]{2,1,0:T(8,128)(2,1)S(1)}, bf16[1,64,2048]{2,1,0:T(8,128)(2,1)S(1)}, u32[]{:S(2)}, u32[]{:S(2)}) %collective-permute-start.4) | collective-permute-done | bytes 262176 | tf_op jit(solution)/shard_map/ppermute | solution.py:120
  33.4 0.1 add_convert_fusion.1
  33.5 1.9 %collective-permute-start.5 = (bf16[64,512]{1,0:T(8,128)(2,1)S(1)}, bf16[64,512]{1,0:T(8,128)(2,1)S(1)}, u32[]{:S(2)}, u32[]{:S(2)}) collective-permute-start(bf16[64,512]{1,0:T(8,128)(2,1)S(1)} %get-tuple-element.19), channel_id=1, source_target_pairs={{0,1},{1,2},{2,3},{3,0},{4,5},{5,6},{6,7},{7,4},{8,9},{9,10},{10,1... | collective-permute-start | bytes 196616 | tf_op jit(solution)/shard_map/ppermute | solution.py:124
  35.3 2.6 %collective-permute-start.6 = (bf16[64,512]{1,0:T(8,128)(2,1)S(1)}, bf16[64,512]{1,0:T(8,128)(2,1)S(1)}, u32[]{:S(2)}, u32[]{:S(2)}) collective-permute-start(bf16[64,512]{1,0:T(8,128)(2,1)S(1)} %get-tuple-element.21), channel_id=1, source_target_pairs={{0,2},{1,3},{2,0},{3,1},{4,6},{5,7},{6,4},{7,5},{8,10},{9,11},{10,... | collective-permute-start | bytes 196616 | tf_op jit(solution)/shard_map/ppermute | solution.py:124
  37.9 1.4 %collective-permute-start.7 = (bf16[64,512]{1,0:T(8,128)(2,1)S(1)}, bf16[64,512]{1,0:T(8,128)(2,1)S(1)}, u32[]{:S(2)}, u32[]{:S(2)}) collective-permute-start(bf16[64,512]{1,0:T(8,128)(2,1)S(1)} %get-tuple-element.20), channel_id=1, source_target_pairs={{0,3},{1,0},{2,1},{3,2},{4,7},{5,4},{6,5},{7,6},{8,11},{9,8},{10,9... | collective-permute-start | bytes 196616 | tf_op jit(solution)/shard_map/ppermute | solution.py:124
  39.3 1.0 %collective-permute-done.5 = bf16[64,512]{1,0:T(8,128)(2,1)S(1)} collective-permute-done((bf16[64,512]{1,0:T(8,128)(2,1)S(1)}, bf16[64,512]{1,0:T(8,128)(2,1)S(1)}, u32[]{:S(2)}, u32[]{:S(2)}) %collective-permute-start.5) | collective-permute-done | bytes 65568 | tf_op jit(solution)/shard_map/ppermute | solution.py:124
  40.2 2.3 %collective-permute-done.6 = bf16[64,512]{1,0:T(8,128)(2,1)S(1)} collective-permute-done((bf16[64,512]{1,0:T(8,128)(2,1)S(1)}, bf16[64,512]{1,0:T(8,128)(2,1)S(1)}, u32[]{:S(2)}, u32[]{:S(2)}) %collective-permute-start.6) | collective-permute-done | bytes 65568 | tf_op jit(solution)/shard_map/ppermute | solution.py:124
  42.5 0.0 collective-permute-done.7
  42.6 0.1 multiply_reduce_fusion
  42.7 9.4 %all_to_all.6 = f32[4,1,64]{2,1,0:T(1,128)S(1)} all-to-all(f32[4,1,64]{2,1,0:T(1,128)S(1)} %broadcast_in_dim.2), channel_id=1, replica_groups=mesh['grp'=2,'ep'=4,'tp'=4] {'tp'}, dimensions={0} | all-to-all | bytes 2048 | tf_op jit(solution)/shard_map/all_to_all | solution.py:166
  52.2 0.0 copy-done.4
  52.2 0.7 %multiply_convert_fusion = bf16[64,512]{1,0:T(8,128)(2,1)} fusion(f32[512]{0:T(512)S(1)} %copy-done.4, f32[64]{0:T(128)S(1)} %add_rsqrt_fusion, bf16[64,512]{1,0:T(8,128)(2,1)S(1)} %collective-permute-done.7, bf16[64,512]{1,0:T(8,128)(2,1)S(1)} %collective-permute-done.6, bf16[64,512]{1,0:T(8,128)(2,1)S(1)} %collective-permute-done.5, ...), kind=kLoop, calls=%fused_computation.5 | loop fusion | flops 327680 | bytes 329988 | tf_op jit(solution)/shard_map/convert_element_type | solution.py:168
  (5 shorter events, 0.1 us)
Async XLA Ops:
  0.0 0.9 %copy-start = (bf16[64,2048]{1,0:T(8,128)(2,1)S(1)}, bf16[64,2048]{1,0:T(8,128)(2,1)}, u32[]{:S(2)}) copy-start(bf16[64,2048]{1,0:T(8,128)(2,1)} %tok_ref) | copy-start | bytes 786436
  1.0 0.7 %copy-start.1 = (f32[2048]{0:T(1024)S(1)}, f32[2048]{0:T(1024)}, u32[]{:S(2)}) copy-start(f32[2048]{0:T(1024)} %param.11) | copy-start | bytes 24580
  1.6 0.7 %copy-start.2 = (s32[64,4]{0,1:T(4,128)S(1)}, s32[64,4]{0,1:T(4,128)}, u32[]{:S(2)}) copy-start(s32[64,4]{0,1:T(4,128)} %param.9) | copy-start | bytes 3076
  2.3 0.7 %copy-start.3 = (f32[64,4]{0,1:T(4,128)S(1)}, f32[64,4]{0,1:T(4,128)}, u32[]{:S(2)}) copy-start(f32[64,4]{0,1:T(4,128)} %param.10) | copy-start | bytes 3076
  3.2 9.7 %collective-permute-start.1 = (bf16[64,2176]{1,0:T(8,128)(2,1)S(1)}, bf16[64,2176]{1,0:T(8,128)(2,1)S(1)}, u32[]{:S(2)}, u32[]{:S(2)}) collective-permute-start(bf16[64,2176]{1,0:T(8,128)(2,1)S(1)} %pack.1.refs_0_), channel_id=1, source_target_pairs={{0,8},{4,12},{8,0},{12,4},{1,9},{5,13},{9,1},{13,5},{2,10},{6,14},... | collective-permute-start | bytes 835592 | tf_op jit(solution)/shard_map/ppermute | solution.py:120
  6.2 11.4 %collective-permute-start = (bf16[64,2176]{1,0:T(8,128)(2,1)S(1)}, bf16[64,2176]{1,0:T(8,128)(2,1)S(1)}, u32[]{:S(2)}, u32[]{:S(2)}) collective-permute-start(bf16[64,2176]{1,0:T(8,128)(2,1)S(1)} %pack.1.refs_0_), channel_id=1, source_target_pairs={{0,4},{4,0},{8,12},{12,8},{1,5},{5,1},{9,13},{13,9},{2,6},{6,2},{1... | collective-permute-start | bytes 835592 | tf_op jit(solution)/shard_map/ppermute | solution.py:120
  12.9 4.7 %collective-permute-start.2 = (bf16[64,2176]{1,0:T(8,128)(2,1)S(1)}, bf16[64,2176]{1,0:T(8,128)(2,1)S(1)}, u32[]{:S(2)}, u32[]{:S(2)}) collective-permute-start(bf16[64,2176]{1,0:T(8,128)(2,1)S(1)} %collective-permute-done.1.refs_2_), channel_id=1, source_target_pairs={{0,4},{4,0},{8,12},{12,8},{1,5},{5,1},{9,13},{13,9},{2,6},{6,2},{1... | collective-permute-start | bytes 835592 | tf_op jit(solution)/shard_map/ppermute | solution.py:120
  17.6 34.6 %copy-start.4 = (f32[512]{0:T(512)S(1)}, f32[512]{0:T(512)}, u32[]{:S(2)}) copy-start(f32[512]{0:T(512)} %param.15) | copy-start | bytes 6148
  22.3 2.2 %collective-permute-start.3 = (bf16[2,64,2048]{2,1,0:T(8,128)(2,1)}, bf16[2,64,2048]{2,1,0:T(8,128)(2,1)S(1)}, u32[]{:S(2)}, u32[]{:S(2)}) collective-permute-start(bf16[2,64,2048]{2,1,0:T(8,128)(2,1)} %get-tuple-element.18), channel_id=1, source_target_pairs={{0,4},{4,0},{8,12},{12,8},{1,5},{5,1},{9,13},{13,9},{2,6},{6,2},{1... | collective-permute-start | bytes 1572872 | tf_op jit(solution)/shard_map/ppermute | solution.py:120
  24.7 8.7 %collective-permute-start.4 = (bf16[1,64,2048]{2,1,0:T(8,128)(2,1)S(1)}, bf16[1,64,2048]{2,1,0:T(8,128)(2,1)S(1)}, u32[]{:S(2)}, u32[]{:S(2)}) collective-permute-start(bf16[1,64,2048]{2,1,0:T(8,128)(2,1)S(1)} %slice.13), channel_id=1, source_target_pairs={{0,8},{4,12},{8,0},{12,4},{1,9},{5,13},{9,1},{13,5},{2,10},{6,14},... | collective-permute-start | bytes 786440 | tf_op jit(solution)/shard_map/ppermute | solution.py:120
  33.5 6.7 %collective-permute-start.5 = (bf16[64,512]{1,0:T(8,128)(2,1)S(1)}, bf16[64,512]{1,0:T(8,128)(2,1)S(1)}, u32[]{:S(2)}, u32[]{:S(2)}) collective-permute-start(bf16[64,512]{1,0:T(8,128)(2,1)S(1)} %get-tuple-element.19), channel_id=1, source_target_pairs={{0,1},{1,2},{2,3},{3,0},{4,5},{5,6},{6,7},{7,4},{8,9},{9,10},{10,1... | collective-permute-start | bytes 196616 | tf_op jit(solution)/shard_map/ppermute | solution.py:124
  35.3 7.2 %collective-permute-start.6 = (bf16[64,512]{1,0:T(8,128)(2,1)S(1)}, bf16[64,512]{1,0:T(8,128)(2,1)S(1)}, u32[]{:S(2)}, u32[]{:S(2)}) collective-permute-start(bf16[64,512]{1,0:T(8,128)(2,1)S(1)} %get-tuple-element.21), channel_id=1, source_target_pairs={{0,2},{1,3},{2,0},{3,1},{4,6},{5,7},{6,4},{7,5},{8,10},{9,11},{10,... | collective-permute-start | bytes 196616 | tf_op jit(solution)/shard_map/ppermute | solution.py:124
  37.9 4.6 %collective-permute-start.7 = (bf16[64,512]{1,0:T(8,128)(2,1)S(1)}, bf16[64,512]{1,0:T(8,128)(2,1)S(1)}, u32[]{:S(2)}, u32[]{:S(2)}) collective-permute-start(bf16[64,512]{1,0:T(8,128)(2,1)S(1)} %get-tuple-element.20), channel_id=1, source_target_pairs={{0,3},{1,0},{2,1},{3,2},{4,7},{5,4},{6,5},{7,6},{8,11},{9,8},{10,9... | collective-permute-start | bytes 196616 | tf_op jit(solution)/shard_map/ppermute | solution.py:124

commit v3 on v2

--- a/solution.py
+++ b/solution.py
@@ -13,7 +13,14 @@
 EPS = 1e-06
 
 
-def pack_kernel(tok_ref, route_ref, weight_ref, gain_ref, out_ref, *, half):
+def pack_kernel(*refs, half):
+    sources, out_ref, targets, sems = refs[:4], refs[4], refs[5:9], refs[9]
+    copies = [pltpu.make_async_copy(a, b, sems.at[i]) for i, (a, b) in enumerate(zip(sources, targets))]
+    for copy in copies:
+        copy.start()
+    for copy in copies:
+        copy.wait()
+    tok_ref, route_ref, weight_ref, gain_ref = targets
     width = tok_ref.shape[1]
     scaled = tok_ref[...].astype(jnp.float32)
     mean = jnp.mean(scaled * scaled, axis=-1, keepdims=True)
@@ -31,12 +38,31 @@
 
 def pack(tokens, routing, route_weight, norm_gain, half):
     rows, width = tokens.shape
+    sources = (tokens, routing.T, route_weight.T, norm_gain.reshape(1, width))
     return pl.pallas_call(
         functools.partial(pack_kernel, half=half),
+        in_specs=[pl.BlockSpec(memory_space=pl.ANY)] * len(sources),
+        out_specs=pl.BlockSpec(memory_space=pltpu.VMEM),
         out_shape=jax.ShapeDtypeStruct((rows, width + 2 * half), jnp.bfloat16),
+        scratch_shapes=[pltpu.VMEM(a.shape, a.dtype) for a in sources]
+        + [pltpu.SemaphoreType.DMA((len(sources),))],
         compiler_params=pltpu.CompilerParams(vmem_limit_bytes=16 * 2**20),
         name="pack",
-    )(tokens, routing.T, route_weight.T, norm_gain.reshape(1, width))
+    )(*[pltpu.with_memory_space_constraint(a, pltpu.HBM) for a in sources])
+
+
+def scale_kernel(mix_ref, gain_ref, out_ref):
+    out_ref[...] = mix_ref[...] * gain_ref[...]
+
+
+def scale(mix, gain):
+    return pl.pallas_call(
+        scale_kernel,
+        out_shape=jax.ShapeDtypeStruct(mix.shape, jnp.float32),
+        compiler_params=pltpu.CompilerParams(vmem_limit_bytes=8 * 2**20),
+        cost_estimate=pl.CostEstimate(flops=2**26, bytes_accessed=8 * mix.size, transcendentals=0),
+        name="scale",
+    )(mix, gain.reshape(1, -1))
 
 
 def moe_kernel(place_ref, *refs, blocks, half, chunk):
@@ -100,7 +126,7 @@
     blocks = len(x_blocks)
     rows = x_blocks[0].shape[0]
     width, hidden = gate_weight.shape[1:]
-    out = jax.ShapeDtypeStruct((blocks // 2, rows, width), jnp.bfloat16)
+    out = pltpu.VMEM((blocks // 2, rows, width), jnp.bfloat16)
     return pl.pallas_call(
         functools.partial(moe_kernel, blocks=blocks, half=half, chunk=min(hidden, 256)),
         in_specs=[pl.BlockSpec(memory_space=pltpu.SMEM)]
@@ -163,9 +189,10 @@
         expert_mix += shift(block(d), "tp", tp_size, d).astype(jnp.float32)
     square = jnp.sum(expert_mix * expert_mix, axis=1)
     copies = jnp.broadcast_to(square, (tp_size,) + square.shape)
-    square_sum = jnp.sum(lax.all_to_all(copies, "tp", 0, 0, tiled=True), axis=0)
+    square_sum = jnp.sum(lax.all_to_all(copies, "tp", 0, 0), axis=0)
+    scaled = scale(expert_mix, out_gain)
     scale_factor = lax.rsqrt(square_sum / model_width + EPS)
-    return (expert_mix * scale_factor[:, None] * out_gain).astype(jnp.bfloat16)
+    return (scaled * scale_factor[:, None]).astype(jnp.bfloat16)
 
 
 def solution(mesh):

time: 53.2 us -> 52.5 us (0.987)
  blocking collectives: 9.44 us -> 0 us
  waiting for transfers between devices: 18.5 us -> 23.7 us
  starting transfers between devices: 11.2 us -> 15.4 us
  local copies, waits for them, and re-layouts: 3.06 us -> 1.34 us
  Pallas kernels: 9.55 us -> 10.7 us
    all_to_all x1 -> x0, blocking collectives: 9.44 us -> none  [on_device(): square_sum = jnp.sum(lax.all_to_all(copies, 'tp', 0, 0, tiled=True), axis=0)]
    all_to_all x0 -> x1, waiting for transfers between devices: none -> 5.48 us  [on_device(): square_sum = jnp.sum(lax.all_to_all(copies, 'tp', 0, 0), axis=0)]
    all_to_all x0 -> x1, starting transfers between devices: none -> 4.14 us  [on_device(): square_sum = jnp.sum(lax.all_to_all(copies, 'tp', 0, 0), axis=0)]
    unnamed x10 -> x4, local copies, waits for them, and re-layouts: 3.01 us -> 0.71 us
    pallas_call x1 -> x2, Pallas kernels: 0.16 us -> 1.17 us  [the longest x1 1.15 us: pack(): pl.pallas_call(functools.partial(pack_kernel, half=half), in_specs=[pl.Bl...]
    broadcast_in_dim x1, local copies, waits for them, and re-layouts: 0.01 us -> 0.58 us  [on_device(): copies = jnp.broadcast_to(square, (tp_size,) + square.shape)]
  transfers between devices with their start and end apart: 8 -> 9, of which waited for: 5 -> 7; matrix products, arithmetic and copies ran while one was open for 0% -> 0% of each run, Pallas kernels for 9% -> 9%
where the time goes in v3:
time: 52.5 us; the launch traced here: 52.3 us
  waiting for transfers between devices  23.7 us (45%)
  starting transfers between devices  15.4 us (29%)
  Pallas kernels  10.7 us (20%)
  local copies, waits for them, and re-layouts  1.34 us (3%)
  other arithmetic  1.07 us (2%)
    ppermute x5, waiting for transfers between devices, swap(): return lax.ppermute(value, axis, [(s, s ^ bit) for s in range(size)])  15.1 us
    ppermute x3, starting transfers between devices, shift(): lax.ppermute(value, axis, [(s, (s + amount) % size) for s in range(size)])  5.8 us
    all_to_all x1, waiting for transfers between devices, on_device(): square_sum = jnp.sum(lax.all_to_all(copies, 'tp', 0, 0), axis=0)  5.48 us
    ppermute x5, starting transfers between devices, swap(): return lax.ppermute(value, axis, [(s, s ^ bit) for s in range(size)])  5.42 us
    pallas_call x1, Pallas kernels, run_experts(): pl.pallas_call(functools.partial(moe_kernel, blocks=blocks, half=half, ch...  4.86 us
    pallas_call x1, Pallas kernels, fetch(): pl.pallas_call(fetch_kernel, in_specs=[pl.BlockSpec(memory_space=pl.ANY)]...  4.69 us
    all_to_all x1, starting transfers between devices, on_device(): square_sum = jnp.sum(lax.all_to_all(copies, 'tp', 0, 0), axis=0)  4.14 us
    ppermute x3, waiting for transfers between devices, shift(): lax.ppermute(value, axis, [(s, (s + amount) % size) for s in range(size)])  3.21 us
  transfers between devices with their start and end apart: 9, of which 7 were waited for; matrix products, arithmetic and copies ran while one was open for 0% of the time, Pallas kernels for 9%

profile of v3, /device:TPU:0, one launch (start us, length us, event | category | flops | bytes accessed | tf_op | source)
XLA Modules:
  0.0 52.3 jit_solution(13221281176137964684)
XLA Ops:
  0.0 1.2 %pack.1.refs_0_ = bf16[64,2176]{1,0:T(8,128)(2,1)S(1)} custom-call(bf16[64,2048]{1,0:T(8,128)(2,1)} %refs_0_, s32[4,64]{1,0:T(4,128)} %bitcast.19, f32[4,64]{1,0:T(4,128)} %bitcast.20, f32[1,2048]{1,0:T(1,128)} %bitcast.17), custom_call_target="tpu_custom_call" | custom-call | tf_op jit(solution)/shard_map/pack/pallas_call | solution.py:42
  1.2 3.1 %collective-permute-start.1 = (bf16[64,2176]{1,0:T(8,128)(2,1)S(1)}, bf16[64,2176]{1,0:T(8,128)(2,1)S(1)}, u32[]{:S(2)}, u32[]{:S(2)}) collective-permute-start(bf16[64,2176]{1,0:T(8,128)(2,1)S(1)} %pack.1.refs_0_), channel_id=1, source_target_pairs={{0,8},{4,12},{8,0},{12,4},{1,9},{5,13},{9,1},{13,5},{2,10},{6,14},... | collective-permute-start | bytes 835592 | tf_op jit(solution)/shard_map/ppermute | solution.py:146
  4.2 0.0 collective-permute-start
  4.2 6.7 %collective-permute-done.1.refs_2_ = bf16[64,2176]{1,0:T(8,128)(2,1)S(1)} collective-permute-done((bf16[64,2176]{1,0:T(8,128)(2,1)S(1)}, bf16[64,2176]{1,0:T(8,128)(2,1)S(1)}, u32[]{:S(2)}, u32[]{:S(2)}) %collective-permute-start.1) | collective-permute-done | bytes 278560 | tf_op jit(solution)/shard_map/ppermute | solution.py:146
  10.9 0.0 collective-permute-start.2
  10.9 4.7 %fetch.1 = (bf16[2,2048,512]{2,1,0:T(8,128)(2,1)S(1)}, bf16[2,2048,512]{2,1,0:T(8,128)(2,1)S(1)}, bf16[2,512,2048]{2,1,0:T(8,128)(2,1)S(1)}) custom-call(bf16[64,2176]{1,0:T(8,128)(2,1)S(1)} %pack.1.refs_0_, bf16[2,2048,512]{2,1,0:T(8,128)(2,1)} %refs_1_.1, bf16[2,2048,512]{2,1,0:T(8,128)(2,1)} %refs_2_.1, bf16[2,512,2048]{2,1,0:T(8,128)(2,1)} %refs_3_.1), custom_call_target="tpu_custom_call" | custom-call | flops 1610612736 | bytes 25165824 | tf_op jit(solution)/shard_map/fetch/pallas_call | solution.py:113
  15.6 0.0 collective-permute-done.refs_1_
  15.6 0.0 collective-permute-done.2.refs_3_
  15.6 0.0 copy-start.1
  15.6 0.7 %copy-done.1 = bf16[64,2176]{1,0:T(8,128)(2,1)} copy-done((bf16[64,2176]{1,0:T(8,128)(2,1)}, bf16[64,2176]{1,0:T(8,128)(2,1)S(1)}, u32[]{:S(2)}) %copy-start.1) | copy-done | bytes 278552
  16.3 0.0 copy-start
  16.3 4.9 %experts.1 = (bf16[2,64,2048]{2,1,0:T(8,128)(2,1)S(1)}, bf16[2,64,2048]{2,1,0:T(8,128)(2,1)S(1)}) custom-call(s32[1]{0:T(128)} %bitcast.place_ref, bf16[64,2176]{1,0:T(8,128)(2,1)S(1)} %pack.1.refs_0_, bf16[64,2176]{1,0:T(8,128)(2,1)S(1)} %collective-permute-done.refs_1_, bf16[64,2176]{1,0:T(8,128)(2,1)S(1)} %collective-permute-done.1.refs_2_, ...), custom_call_target="tpu_custom_call" | custom-call | tf_op jit(solution)/shard_map/experts/pallas_call | solution.py:130
  21.2 0.6 %collective-permute-start.3 = (bf16[2,64,2048]{2,1,0:T(8,128)(2,1)S(1)}, bf16[2,64,2048]{2,1,0:T(8,128)(2,1)S(1)}, u32[]{:S(2)}, u32[]{:S(2)}) collective-permute-start(bf16[2,64,2048]{2,1,0:T(8,128)(2,1)S(1)} %get-tuple-element.18), channel_id=1, source_target_pairs={{0,4},{4,0},{8,12},{12,8},{1,5},{5,1},{9,13},{13,9},{2,6},{6,2},{1... | collective-permute-start | bytes 1572872 | tf_op jit(solution)/shard_map/ppermute | solution.py:146
  21.7 1.5 %collective-permute-done.3 = bf16[2,64,2048]{2,1,0:T(8,128)(2,1)S(1)} collective-permute-done((bf16[2,64,2048]{2,1,0:T(8,128)(2,1)S(1)}, bf16[2,64,2048]{2,1,0:T(8,128)(2,1)S(1)}, u32[]{:S(2)}, u32[]{:S(2)}) %collective-permute-start.3) | collective-permute-done | bytes 524320 | tf_op jit(solution)/shard_map/ppermute | solution.py:146
  23.3 0.1 add_convert_fusion
  23.4 1.8 %collective-permute-start.4 = (bf16[1,64,2048]{2,1,0:T(8,128)(2,1)S(1)}, bf16[1,64,2048]{2,1,0:T(8,128)(2,1)S(1)}, u32[]{:S(2)}, u32[]{:S(2)}) collective-permute-start(bf16[1,64,2048]{2,1,0:T(8,128)(2,1)S(1)} %slice.13), channel_id=1, source_target_pairs={{0,8},{4,12},{8,0},{12,4},{1,9},{5,13},{9,1},{13,5},{2,10},{6,14},... | collective-permute-start | bytes 786440 | tf_op jit(solution)/shard_map/ppermute | solution.py:146
  25.2 6.9 %collective-permute-done.4 = bf16[1,64,2048]{2,1,0:T(8,128)(2,1)S(1)} collective-permute-done((bf16[1,64,2048]{2,1,0:T(8,128)(2,1)S(1)}, bf16[1,64,2048]{2,1,0:T(8,128)(2,1)S(1)}, u32[]{:S(2)}, u32[]{:S(2)}) %collective-permute-start.4) | collective-permute-done | bytes 262176 | tf_op jit(solution)/shard_map/ppermute | solution.py:146
  32.1 0.1 add_convert_fusion.1
  32.2 1.9 %collective-permute-start.5 = (bf16[64,512]{1,0:T(8,128)(2,1)S(1)}, bf16[64,512]{1,0:T(8,128)(2,1)S(1)}, u32[]{:S(2)}, u32[]{:S(2)}) collective-permute-start(bf16[64,512]{1,0:T(8,128)(2,1)S(1)} %get-tuple-element.21), channel_id=1, source_target_pairs={{0,1},{1,2},{2,3},{3,0},{4,5},{5,6},{6,7},{7,4},{8,9},{9,10},{10,1... | collective-permute-start | bytes 196616 | tf_op jit(solution)/shard_map/ppermute | solution.py:150
  34.0 2.6 %collective-permute-start.6 = (bf16[64,512]{1,0:T(8,128)(2,1)S(1)}, bf16[64,512]{1,0:T(8,128)(2,1)S(1)}, u32[]{:S(2)}, u32[]{:S(2)}) collective-permute-start(bf16[64,512]{1,0:T(8,128)(2,1)S(1)} %get-tuple-element.23), channel_id=1, source_target_pairs={{0,2},{1,3},{2,0},{3,1},{4,6},{5,7},{6,4},{7,5},{8,10},{9,11},{10,... | collective-permute-start | bytes 196616 | tf_op jit(solution)/shard_map/ppermute | solution.py:150
  36.6 1.4 %collective-permute-start.7 = (bf16[64,512]{1,0:T(8,128)(2,1)S(1)}, bf16[64,512]{1,0:T(8,128)(2,1)S(1)}, u32[]{:S(2)}, u32[]{:S(2)}) collective-permute-start(bf16[64,512]{1,0:T(8,128)(2,1)S(1)} %get-tuple-element.22), channel_id=1, source_target_pairs={{0,3},{1,0},{2,1},{3,2},{4,7},{5,4},{6,5},{7,6},{8,11},{9,8},{10,9... | collective-permute-start | bytes 196616 | tf_op jit(solution)/shard_map/ppermute | solution.py:150
  38.0 0.8 %collective-permute-done.5 = bf16[64,512]{1,0:T(8,128)(2,1)S(1)} collective-permute-done((bf16[64,512]{1,0:T(8,128)(2,1)S(1)}, bf16[64,512]{1,0:T(8,128)(2,1)S(1)}, u32[]{:S(2)}, u32[]{:S(2)}) %collective-permute-start.5) | collective-permute-done | bytes 65568 | tf_op jit(solution)/shard_map/ppermute | solution.py:150
  38.8 2.3 %collective-permute-done.6 = bf16[64,512]{1,0:T(8,128)(2,1)S(1)} collective-permute-done((bf16[64,512]{1,0:T(8,128)(2,1)S(1)}, bf16[64,512]{1,0:T(8,128)(2,1)S(1)}, u32[]{:S(2)}, u32[]{:S(2)}) %collective-permute-start.6) | collective-permute-done | bytes 65568 | tf_op jit(solution)/shard_map/ppermute | solution.py:150
  41.1 0.1 collective-permute-done.7
  41.2 0.1 multiply_reduce_fusion
  41.3 0.6 %broadcast_in_dim.4 = f32[4,1,64]{2,1,0:T(1,128)} broadcast(f32[64]{0:T(128)S(1)} %get-tuple-element.19), dimensions={2} | broadcast | bytes 1280 | tf_op jit(solution)/shard_map/broadcast_in_dim | solution.py:191
  41.9 4.1 %all-to-all-start = ((f32[4,1,64]{2,1,0:T(1,128)}), f32[4,1,64]{2,1,0:T(1,128)S(1)}, u32[]{:S(2)}, u32[]{:S(2)}) async-start(f32[4,1,64]{2,1,0:T(1,128)} %broadcast_in_dim.4), calls=%async_computation | async-start | bytes 4096 | tf_op jit(solution)/shard_map/all_to_all | solution.py:192
  46.1 0.0 copy-done
  46.1 5.5 %all-to-all-done = f32[4,1,64]{2,1,0:T(1,128)S(1)} async-done(((f32[4,1,64]{2,1,0:T(1,128)}), f32[4,1,64]{2,1,0:T(1,128)S(1)}, u32[]{:S(2)}, u32[]{:S(2)}) %all-to-all-start) | async-done | bytes 1056 | tf_op jit(solution)/shard_map/all_to_all | solution.py:192
  51.6 0.7 %multiply_convert_fusion = bf16[64,512]{1,0:T(8,128)(2,1)} fusion(f32[64,512]{1,0:T(8,128)S(1)} %scale.1, f32[64]{0:T(128)S(1)} %add_rsqrt_fusion), kind=kLoop, calls=%fused_computation.5 | loop fusion | flops 65536 | bytes 196864 | tf_op jit(solution)/shard_map/convert_element_type | solution.py:195
  (5 shorter events, 0.1 us)
Async XLA Ops:
  1.2 9.7 %collective-permute-start.1 = (bf16[64,2176]{1,0:T(8,128)(2,1)S(1)}, bf16[64,2176]{1,0:T(8,128)(2,1)S(1)}, u32[]{:S(2)}, u32[]{:S(2)}) collective-permute-start(bf16[64,2176]{1,0:T(8,128)(2,1)S(1)} %pack.1.refs_0_), channel_id=1, source_target_pairs={{0,8},{4,12},{8,0},{12,4},{1,9},{5,13},{9,1},{13,5},{2,10},{6,14},... | collective-permute-start | bytes 835592 | tf_op jit(solution)/shard_map/ppermute | solution.py:146
  4.2 11.4 %collective-permute-start = (bf16[64,2176]{1,0:T(8,128)(2,1)S(1)}, bf16[64,2176]{1,0:T(8,128)(2,1)S(1)}, u32[]{:S(2)}, u32[]{:S(2)}) collective-permute-start(bf16[64,2176]{1,0:T(8,128)(2,1)S(1)} %pack.1.refs_0_), channel_id=1, source_target_pairs={{0,4},{4,0},{8,12},{12,8},{1,5},{5,1},{9,13},{13,9},{2,6},{6,2},{1... | collective-permute-start | bytes 835592 | tf_op jit(solution)/shard_map/ppermute | solution.py:146
  10.9 4.7 %collective-permute-start.2 = (bf16[64,2176]{1,0:T(8,128)(2,1)S(1)}, bf16[64,2176]{1,0:T(8,128)(2,1)S(1)}, u32[]{:S(2)}, u32[]{:S(2)}) collective-permute-start(bf16[64,2176]{1,0:T(8,128)(2,1)S(1)} %collective-permute-done.1.refs_2_), channel_id=1, source_target_pairs={{0,4},{4,0},{8,12},{12,8},{1,5},{5,1},{9,13},{13,9},{2,6},{6,2},{1... | collective-permute-start | bytes 835592 | tf_op jit(solution)/shard_map/ppermute | solution.py:146
  15.6 0.7 %copy-start.1 = (bf16[64,2176]{1,0:T(8,128)(2,1)}, bf16[64,2176]{1,0:T(8,128)(2,1)S(1)}, u32[]{:S(2)}) copy-start(bf16[64,2176]{1,0:T(8,128)(2,1)S(1)} %collective-permute-done.2.refs_3_) | copy-start | bytes 835588
  16.3 29.8 %copy-start = (f32[512]{0:T(512)S(1)}, f32[512]{0:T(512)}, u32[]{:S(2)}) copy-start(f32[512]{0:T(512)} %param.15) | copy-start | bytes 6148
  21.2 2.1 %collective-permute-start.3 = (bf16[2,64,2048]{2,1,0:T(8,128)(2,1)S(1)}, bf16[2,64,2048]{2,1,0:T(8,128)(2,1)S(1)}, u32[]{:S(2)}, u32[]{:S(2)}) collective-permute-start(bf16[2,64,2048]{2,1,0:T(8,128)(2,1)S(1)} %get-tuple-element.18), channel_id=1, source_target_pairs={{0,4},{4,0},{8,12},{12,8},{1,5},{5,1},{9,13},{13,9},{2,6},{6,2},{1... | collective-permute-start | bytes 1572872 | tf_op jit(solution)/shard_map/ppermute | solution.py:146
  23.4 8.7 %collective-permute-start.4 = (bf16[1,64,2048]{2,1,0:T(8,128)(2,1)S(1)}, bf16[1,64,2048]{2,1,0:T(8,128)(2,1)S(1)}, u32[]{:S(2)}, u32[]{:S(2)}) collective-permute-start(bf16[1,64,2048]{2,1,0:T(8,128)(2,1)S(1)} %slice.13), channel_id=1, source_target_pairs={{0,8},{4,12},{8,0},{12,4},{1,9},{5,13},{9,1},{13,5},{2,10},{6,14},... | collective-permute-start | bytes 786440 | tf_op jit(solution)/shard_map/ppermute | solution.py:146
  32.2 6.6 %collective-permute-start.5 = (bf16[64,512]{1,0:T(8,128)(2,1)S(1)}, bf16[64,512]{1,0:T(8,128)(2,1)S(1)}, u32[]{:S(2)}, u32[]{:S(2)}) collective-permute-start(bf16[64,512]{1,0:T(8,128)(2,1)S(1)} %get-tuple-element.21), channel_id=1, source_target_pairs={{0,1},{1,2},{2,3},{3,0},{4,5},{5,6},{6,7},{7,4},{8,9},{9,10},{10,1... | collective-permute-start | bytes 196616 | tf_op jit(solution)/shard_map/ppermute | solution.py:150
  34.0 7.1 %collective-permute-start.6 = (bf16[64,512]{1,0:T(8,128)(2,1)S(1)}, bf16[64,512]{1,0:T(8,128)(2,1)S(1)}, u32[]{:S(2)}, u32[]{:S(2)}) collective-permute-start(bf16[64,512]{1,0:T(8,128)(2,1)S(1)} %get-tuple-element.23), channel_id=1, source_target_pairs={{0,2},{1,3},{2,0},{3,1},{4,6},{5,7},{6,4},{7,5},{8,10},{9,11},{10,... | collective-permute-start | bytes 196616 | tf_op jit(solution)/shard_map/ppermute | solution.py:150
  36.6 4.6 %collective-permute-start.7 = (bf16[64,512]{1,0:T(8,128)(2,1)S(1)}, bf16[64,512]{1,0:T(8,128)(2,1)S(1)}, u32[]{:S(2)}, u32[]{:S(2)}) collective-permute-start(bf16[64,512]{1,0:T(8,128)(2,1)S(1)} %get-tuple-element.22), channel_id=1, source_target_pairs={{0,3},{1,0},{2,1},{3,2},{4,7},{5,4},{6,5},{7,6},{8,11},{9,8},{10,9... | collective-permute-start | bytes 196616 | tf_op jit(solution)/shard_map/ppermute | solution.py:150
  41.9 9.6 %all-to-all-start = ((f32[4,1,64]{2,1,0:T(1,128)}), f32[4,1,64]{2,1,0:T(1,128)S(1)}, u32[]{:S(2)}, u32[]{:S(2)}) async-start(f32[4,1,64]{2,1,0:T(1,128)} %broadcast_in_dim.4), calls=%async_computation | async-start | bytes 4096 | tf_op jit(solution)/shard_map/all_to_all | solution.py:192
